TPU v7x, 512 devices: a whole 4x4x16 slice. The times are simulated.
512 devices in a mesh: sp: 64 (over z, y), tp: 8 (over x, core).
Axes of the slice: x: 4, y: 4, z: 16, core: 2. Of those that a mesh axis runs over, the one named last changes fastest.
Arguments:
- latent: bfloat16 [16384, 2048], P(('sp', 'tp')), may hold values from -3 to 3
- context: bfloat16 [1024, 2048], P('sp'), may hold values from -6 to 6
- condition: float32 [2048], replicated, may hold values from -6 to 6
- ctx_cond: float32 [2048], replicated, may hold values from -6 to 6
- norm_gain: float32 [2048], replicated, may hold values from 0.1 to 1.9
- w_shift: bfloat16 [2048, 2048], P('sp', 'tp'), may hold values from -0.25 to 0.25
- w_scale: bfloat16 [2048, 2048], P('sp', 'tp'), may hold values from -0.25 to 0.25
- w_gate: bfloat16 [2048, 2048], P('sp', 'tp'), may hold values from -0.25 to 0.25
- w_query: bfloat16 [2048, 2048], P(None, 'tp'), may hold values from -0.125 to 0.125
- w_key: bfloat16 [2048, 2048], P(None, 'tp'), may hold values from -0.125 to 0.125
- w_value: bfloat16 [2048, 2048], P(None, 'tp'), may hold values from -0.125 to 0.125
- w_out: bfloat16 [2048, 2048], P('tp'), may hold values from -0.125 to 0.125
- rel_bias: float32 [16, 15, 31], replicated, may hold values from 2 to 250
Outputs:
- updated: bfloat16 [16384, 2048], P(('sp', 'tp'))
All inputs are finite; a program needn't handle non-finite values.
Results may differ from a plain program's by a relative error of at most 0.015.
Values may be sent and summed in bfloat16 or wider, within the bound.
A program may use at most 64 MiB of HBM per device.

v0:
```python
import jax
import jax.numpy as jnp
from jax import lax
from jax.sharding import Mesh
from jax.sharding import PartitionSpec as P

HEADS = 16
HEAD_DIM = 128
GRID_W = 32
WIN_H = 8
WIN_W = 16
SP = ("sp_0", "sp_1")
SP_TP = ("sp_0", "sp_1", "tp")


NORM_EPS = 1e-06
NEG_BIG = -1e30


def one_axis_at_a_time(array, axes):
    for axis in axes:
        array = lax.psum(array, axis)
    return array


def sent_to_all(array, axis):
    size = lax.axis_size(axis)
    return lax.all_to_all(
        jnp.broadcast_to(array[None], (size, *array.shape)), axis, 0, 0, tiled=True
    )


def joined_along(parts, dim):
    parts = jnp.moveaxis(parts, 0, dim)
    dims = parts.shape
    return parts.reshape(*dims[:dim], dims[dim] * dims[dim + 1], *dims[dim + 2 :])


def collect(array, axis, dim):
    parts = sent_to_all(array, axis)
    return joined_along(parts, dim)


def gathered_by_axis(array, axes, dim):
    whole = array
    for number in range(len(axes) - 1, -1, -1):
        whole = lax.all_gather(whole, axes[number], axis=dim, tiled=True)
    return whole


def padded_2(cells, sides, width):
    for axis, dim in sides:
        count = lax.axis_size(axis)
        ends = count - 1
        head = lax.slice_in_dim(cells, 0, width, axis=dim)
        tail = lax.slice_in_dim(cells, cells.shape[dim] - width, cells.shape[dim], axis=dim)
        cells = jnp.concatenate(
            [
                lax.ppermute(tail, axis, [(i, (i + 1) % count) for i in range(ends)]),
                cells,
                lax.ppermute(head, axis, [((i + 1) % count, i) for i in range(ends)]),
            ],
            axis=dim,
        )
    return cells


def in_blocks(array, dim, size):
    dims = array.shape
    parts = array.reshape(*dims[:dim], size, dims[dim] // size, *dims[dim + 1 :])
    return jnp.moveaxis(parts, dim, 0)


def summed_on_arrival(array, axis, dim):
    parts = in_blocks(array, dim, lax.axis_size(axis))
    arrived = lax.all_to_all(parts, axis, split_axis=0, concat_axis=0, tiled=True)
    return arrived.astype(jnp.float32).sum(axis=0)


def rms_mod(block, norm_gain, shifts, scales):
    block = block.astype(jnp.float32)
    normed = (
        block * lax.rsqrt(jnp.mean(block * block, axis=-1, keepdims=True) + NORM_EPS) * norm_gain
    )
    return (normed * (1.0 + scales) + shifts).astype(jnp.bfloat16)


def project(block, weights):
    return jnp.stack(
        [
            jnp.dot(block, weight, preferred_element_type=jnp.float32).astype(jnp.bfloat16)
            for weight in weights
        ]
    )


def on_device(
    latent,
    context,
    condition,
    ctx_cond,
    norm_gain,
    w_shift,
    w_scale,
    w_gate,
    w_query,
    w_key,
    w_value,
    w_out,
    rel_bias,
):
    tp_size = lax.axis_size("tp")
    sp_size = lax.axis_size(SP)
    head_dev = HEADS // tp_size
    head_cols = w_query.shape[1]
    row_part = w_shift.shape[0]
    activated = jax.nn.silu(jnp.stack([condition, ctx_cond])).astype(jnp.bfloat16)
    act_rows = lax.dynamic_slice_in_dim(activated, lax.axis_index(SP) * row_part, row_part, 1)
    partial_value = jnp.concatenate(
        [
            jnp.dot(act_rows, w_shift, preferred_element_type=jnp.float32),
            jnp.dot(act_rows, w_scale, preferred_element_type=jnp.float32),
            jnp.dot(act_rows[:1], w_gate, preferred_element_type=jnp.float32),
        ],
        axis=0,
    )
    summed = one_axis_at_a_time(partial_value, SP)
    mod_vecs = collect(summed, "tp", 1)
    normed = rms_mod(latent, norm_gain, mod_vecs[0], mod_vecs[2])
    projected = project(collect(normed, "tp", 0), (w_query, w_key, w_value))
    ctx_kv = gathered_by_axis(
        project(rms_mod(context, norm_gain, mod_vecs[1], mod_vecs[3]), (w_key, w_value)), SP, 1
    )
    ctx_key3 = ctx_kv[0].reshape(-1, head_dev, HEAD_DIM)
    ctx_val3 = ctx_kv[1].reshape(-1, head_dev, HEAD_DIM)
    grid_rows = projected.shape[1] // GRID_W
    queries = projected[0].reshape(grid_rows, GRID_W, head_dev, HEAD_DIM)
    half_win = WIN_H // 2
    padded = padded_2(projected[1:].reshape(2, grid_rows, GRID_W, head_cols), ((SP, 1),), half_win)
    total_rows = grid_rows * sp_size
    first_row = lax.axis_index(SP) * grid_rows
    local_rows = jnp.arange(grid_rows, dtype=jnp.int32)
    starts = (
        jnp.clip(first_row + local_rows - half_win, 0, total_rows - WIN_H) - first_row + half_win
    )

    def take_window(start_row):
        return lax.dynamic_slice_in_dim(padded, start_row, WIN_H, 1)

    windows = jax.vmap(take_window)(starts)
    key_win = windows[:, 0].reshape(grid_rows, WIN_H, GRID_W, head_dev, HEAD_DIM)
    val_win = windows[:, 1].reshape(grid_rows, WIN_H, GRID_W, head_dev, HEAD_DIM)
    row_off = (
        starts[:, None]
        - half_win
        + jnp.arange(WIN_H, dtype=jnp.int32)[None, :]
        - local_rows[:, None]
        + WIN_H
        - 1
    )
    col_ids = jnp.arange(GRID_W, dtype=jnp.int32)
    col_start = jnp.clip(col_ids - WIN_W // 2, 0, GRID_W - WIN_W)
    col_in = (col_ids[None, :] >= col_start[:, None]) & (
        col_ids[None, :] < col_start[:, None] + WIN_W
    )
    col_off = jnp.clip(col_ids[None, :] - col_ids[:, None], 1 - WIN_W, WIN_W - 1) + WIN_W - 1
    col_hot = (col_off[:, :, None] == jnp.arange(2 * WIN_W - 1)[None, None, :]).astype(jnp.float32)
    row_hot = (row_off[:, :, None] == jnp.arange(2 * WIN_H - 1)[None, None, :]).astype(jnp.float32)
    bias_table = lax.dynamic_slice_in_dim(rel_bias, lax.axis_index("tp") * head_dev, head_dev, 0)
    col_table = jnp.einsum("hec,qwc->heqw", bias_table, col_hot, precision=lax.Precision.HIGHEST)
    bias_win = jnp.einsum("rke,heqw->rqhkw", row_hot, col_table, precision=lax.Precision.HIGHEST)
    inv_scale = HEAD_DIM ** (-0.5)
    scores_win = (
        jnp.einsum("rqhd,rkwhd->rqhkw", queries, key_win, preferred_element_type=jnp.float32)
        * inv_scale
        + bias_win
    )
    scores_win = jnp.where(col_in[None, :, None, None, :], scores_win, NEG_BIG)
    scores_win = scores_win.reshape(grid_rows, GRID_W, head_dev, WIN_H * GRID_W)
    scores_ctx = (
        jnp.einsum("rqhd,chd->rqhc", queries, ctx_key3, preferred_element_type=jnp.float32)
        * inv_scale
    )
    row_max = jnp.maximum(jnp.max(scores_win, axis=-1), jnp.max(scores_ctx, axis=-1))
    exp_win = jnp.exp(scores_win - row_max[..., None])
    exp_ctx = jnp.exp(scores_ctx - row_max[..., None])
    row_total = jnp.sum(exp_win, axis=-1) + jnp.sum(exp_ctx, axis=-1)
    probs_win = (exp_win / row_total[..., None]).astype(jnp.bfloat16)
    probs_win = probs_win.reshape(grid_rows, GRID_W, head_dev, WIN_H, GRID_W)
    probs_ctx = (exp_ctx / row_total[..., None]).astype(jnp.bfloat16)
    attended = jnp.einsum(
        "rqhkw,rkwhd->rqhd", probs_win, val_win, preferred_element_type=jnp.float32
    )
    attended = attended + jnp.einsum(
        "rqhc,chd->rqhd", probs_ctx, ctx_val3, preferred_element_type=jnp.float32
    )
    attended = attended.astype(jnp.bfloat16).reshape(grid_rows * GRID_W, head_cols)
    branch = summed_on_arrival(
        jnp.dot(attended, w_out, preferred_element_type=jnp.float32).astype(jnp.bfloat16), "tp", 0
    )
    return (latent.astype(jnp.float32) + mod_vecs[4] * branch).astype(jnp.bfloat16)


def solution(mesh):
    torus = Mesh(mesh.devices.reshape(16, 4, mesh.shape["tp"]), ("sp_0", "sp_1", "tp"))
    return jax.shard_map(
        on_device,
        mesh=torus,
        in_specs=(
            P(SP_TP, None),
            P(SP, None),
            P(),
            P(),
            P(),
            P(SP, "tp"),
            P(SP, "tp"),
            P(SP, "tp"),
            P(None, "tp"),
            P(None, "tp"),
            P(None, "tp"),
            P("tp", None),
            P(),
        ),
        out_specs=P(SP_TP, None),
        check_vma=False,
    )
```

profile of v0, /device:TPU:1, one launch (start us, length us, event | category | flops | bytes accessed | tf_op | source)
XLA Modules:
  0.0 196.9 jit_solution(1419718682703808817)
XLA Ops:
  9.9 30.8 %psum.14 = f32[5,256]{1,0:T(8,128)S(1)} all-reduce(f32[5,256]{1,0:T(8,128)S(1)} %pad_maximum_fusion.3), channel_id=1, replica_groups=mesh['sp_0'=16,'sp_1'=4,'tp'=8] {'sp_0'}, use_global_device_ids=true, to_apply=%region_0.1 | all-reduce | flops 1280 | bytes 10240 | tf_op jit(solution)/shard_map/psum | solution.py:22
  40.7 8.8 %psum.15 = f32[5,256]{1,0:T(8,128)S(1)} all-reduce(f32[5,256]{1,0:T(8,128)S(1)} %psum.14), channel_id=1, replica_groups=mesh['sp_0'=16,'sp_1'=4,'tp'=8] {'sp_1'}, use_global_device_ids=true, to_apply=%region_1.2 | all-reduce | flops 1280 | bytes 10240 | tf_op jit(solution)/shard_map/psum | solution.py:22
  50.2 14.0 %all-to-all-start = ((f32[8,5,256]{2,1,0:T(8,128)}), f32[8,5,256]{2,1,0:T(8,128)S(1)}, u32[]{:S(2)}, u32[]{:S(2)}) async-start(f32[8,5,256]{2,1,0:T(8,128)} %broadcast_in_dim.12), calls=%async_computation | async-start | bytes 131072 | tf_op jit(solution)/shard_map/all_to_all | solution.py:28
  67.2 1.4 convolution_bitcast_fusion
  69.7 2.2 %copy.76 = f32[2,32,32,8,8]{1,2,4,0,3:T(8,128)} copy(f32[2,32,32,8,8]{2,4,3,1,0:T(8,128)S(1)} %fusion.34) | data formatting | bytes 1048576 | tf_op jit(solution)/shard_map/rke,heqw->rqhkw/dot_general | solution.py:171
  72.0 1.1 broadcast_in_dim.13
  73.2 4.8 %all-to-all-start.1 = ((bf16[8,32,2048]{2,1,0:T(8,128)(2,1)}), bf16[8,32,2048]{2,1,0:T(8,128)(2,1)S(1)}, u32[]{:S(2)}, u32[]{:S(2)}) async-start(bf16[8,32,2048]{2,1,0:T(8,128)(2,1)} %broadcast_in_dim.13), calls=%async_computation.1 | async-start | bytes 2097152 | tf_op jit(solution)/shard_map/all_to_all | solution.py:28
  78.3 1.5 fusion.7
  79.8 10.1 %all_gather.6 = bf16[2,64,256]{2,1,0:T(8,128)(2,1)} all-gather(bf16[2,16,256]{2,1,0:T(8,128)(2,1)S(1)} %pad_maximum_fusion.2), channel_id=1, replica_groups=mesh['sp_0'=16,'sp_1'=4,'tp'=8] {'sp_1'}, dimensions={1}, use_global_device_ids=true | all-gather | bytes 81920 | tf_op jit(solution)/shard_map/all_gather | solution.py:47
  89.9 3.0 %all-to-all-done.1 = bf16[8,32,2048]{2,1,0:T(8,128)(2,1)S(1)} async-done(((bf16[8,32,2048]{2,1,0:T(8,128)(2,1)}), bf16[8,32,2048]{2,1,0:T(8,128)(2,1)S(1)}, u32[]{:S(2)}, u32[]{:S(2)}) %all-to-all-start.1) | async-done | bytes 1048608 | tf_op jit(solution)/shard_map/all_to_all | solution.py:28
  94.6 1.3 collective-permute-start
  95.9 1.3 collective-permute-start.1
  99.1 2.7 %collective-permute-done.1 = bf16[2,4,32,256]{3,2,0,1:T(8,128)(2,1)} collective-permute-done((bf16[2,4,32,256]{3,2,0,1:T(8,128)(2,1)S(1)}, bf16[2,4,32,256]{3,2,0,1:T(8,128)(2,1)}, u32[]{:S(2)}, u32[]{:S(2)}) %collective-permute-start.1) | collective-permute-done | bytes 131104 | tf_op jit(solution)/shard_map/ppermute | solution.py:61
  102.8 2.0 %gather_fusion = bf16[8,2,8,32,256]{4,3,1,2,0:T(8,128)(2,1)} fusion(bf16[2,16,32,256]{3,2,0,1:T(8,128)(2,1)S(1)} %pad_maximum_fusion, s32[8]{0:T(128)S(1)} %shift-left_bitcast_fusion), kind=kCustom, calls=%fused_computation | custom fusion | bytes 4194432 | tf_op jit(solution)/shard_map/vmap()/gather | solution.py:148
  104.8 3.1 %fusion.46 = (bf16[8,1,8,32,256]{4,3,1,2,0:T(8,128)(2,1)}, bf16[8,1,8,32,256]{4,3,1,2,0:T(8,128)(2,1)}) fusion(bf16[8,2,8,32,256]{4,3,1,2,0:T(8,128)(2,1)} %gather_fusion), kind=kLoop, calls=%fused_computation.92 | loop fusion | bytes 4194304 | tf_op jit(solution)/shard_map/slice | solution.py:151
  107.9 2.3 %reshape_squeeze.13 = bf16[8,8,32,2,128]{4,3,2,1,0:T(2,128)(2,1)} reshape(bf16[8,1,8,32,256]{4,3,1,2,0:T(8,128)(2,1)} %get-tuple-element.5) | data formatting | bytes 2097152 | tf_op jit(solution)/shard_map/reshape;squeeze | solution.py:151
  110.2 2.2 %reshape_squeeze.12 = bf16[8,8,32,2,128]{4,3,2,1,0:T(2,128)(2,1)} reshape(bf16[8,1,8,32,256]{4,3,1,2,0:T(8,128)(2,1)} %get-tuple-element.6) | data formatting | bytes 2097152 | tf_op jit(solution)/shard_map/reshape;squeeze | solution.py:152
  112.4 3.2 %fusion.49 = (f32[8,32,2]{1,2,0:T(2,128)S(1)}, f32[8,32,2,8,32]{1,4,3,2,0:T(8,128)}) fusion(f32[2,32,32,8,8]{1,2,4,0,3:T(8,128)S(1)} %copy-done.1, bf16[8,32,2,128,1]{3,2,1,0,4:T(2,128)(2,1)S(1)} %bitcast.118, bf16[8,8,32,2,128]{4,3,2,1,0:T(2,128)(2,1)} %reshape_squeeze.13, pred[32,32]{0,1:T(8,128)(4,1)S(1)} %fusion.37), kind=kOutput, calls=%fused_computation.95 | convolution fusion | flops 34078208 | bytes 2231296 | tf_op jit(solution)/shard_map/rqhd,rkwhd->rqhkw/dot_general | solution.py:174
  115.5 31.5 %all-gather.2.cloned.1.call-done = bf16[2,1024,256]{2,1,0:T(8,128)(2,1)} async-done(((bf16[2,64,256]{2,1,0:T(8,128)(2,1)}), bf16[2,1024,256]{2,1,0:T(8,128)(2,1)}) %all-gather.2.cloned.1.call-update) | async-done | bytes 1048592 | tf_op jit(solution)/shard_map/all_gather | solution.py:47
  147.0 2.1 %fusion.47 = (bf16[1,1024,256]{2,1,0:T(8,128)(2,1)}, bf16[1,1024,256]{2,1,0:T(8,128)(2,1)S(1)}) fusion(bf16[2,1024,256]{2,1,0:T(8,128)(2,1)} %all-gather.2.cloned.1.call-done), kind=kLoop, calls=%fused_computation.93 | loop fusion | bytes 2097152 | tf_op jit(solution)/shard_map/slice | solution.py:135
  150.0 1.5 fusion.13
  153.5 2.0 %reshape_squeeze.15 = bf16[1024,2,128]{2,1,0:T(2,128)(2,1)} reshape(bf16[1,1024,256]{2,1,0:T(8,128)(2,1)} %get-tuple-element.7) | data formatting | bytes 1048576 | tf_op jit(solution)/shard_map/reshape;squeeze | solution.py:135
  155.5 2.5 %convolution_bitcast_fusion.2 = f32[8,32,2,128]{3,1,2,0:T(8,128)S(1)} fusion(bf16[8,8,32,2,128]{4,3,2,1,0:T(2,128)(2,1)} %reshape_squeeze.12, f32[8,32,2,8,32]{1,4,3,2,0:T(8,128)} %get-tuple-element.17, f32[8,32,2]{1,2,0:T(2,128)S(1)} %copy.82, f32[8,32,2]{1,2,0:T(2,128)S(1)} %copy.80), kind=kOutput, calls=%fused_computation.16 | convolution fusion | flops 33947648 | bytes 1839104 | tf_op jit(solution)/shard_map/rqhkw,rkwhd->rqhd/dot_general | solution.py:191
  159.2 30.0 %all_to_all.15 = bf16[8,32,2048]{2,1,0:T(8,128)(2,1)S(1)} all-to-all(bf16[8,32,2048]{2,1,0:T(8,128)(2,1)S(1)} %bitcast.117), channel_id=1, replica_groups=mesh['sp_0'=16,'sp_1'=4,'tp'=8] {'tp'}, dimensions={0} | all-to-all | bytes 2097152 | tf_op jit(solution)/shard_map/all_to_all | solution.py:76
  (70 shorter events, 18.0 us)
Async XLA Ops:
  6.5 152.2 %copy-start = (bf16[256,2048]{1,0:T(8,128)(2,1)S(1)}, bf16[256,2048]{1,0:T(8,128)(2,1)}, u32[]{:S(2)}) copy-start(bf16[256,2048]{1,0:T(8,128)(2,1)} %param.24) | copy-start | bytes 3145732
  50.2 21.7 %all-to-all-start = ((f32[8,5,256]{2,1,0:T(8,128)}), f32[8,5,256]{2,1,0:T(8,128)S(1)}, u32[]{:S(2)}, u32[]{:S(2)}) async-start(f32[8,5,256]{2,1,0:T(8,128)} %broadcast_in_dim.12), calls=%async_computation | async-start | bytes 131072 | tf_op jit(solution)/shard_map/all_to_all | solution.py:28
  69.6 2.3 %copy-start.5 = (bf16[32,2048]{1,0:T(8,128)(2,1)S(1)}, bf16[32,2048]{1,0:T(8,128)(2,1)}, u32[]{:S(2)}) copy-start(bf16[32,2048]{1,0:T(8,128)(2,1)} %param.13) | copy-start | bytes 393220
  69.6 2.3 %copy-start.11 = (f32[2048]{0:T(1024)S(1)}, f32[2048]{0:T(1024)}, u32[]{:S(2)}) copy-start(f32[2048]{0:T(1024)} %param.17) | copy-start | bytes 24580
  71.8 6.1 %copy-start.3 = (bf16[2048,256]{1,0:T(8,128)(2,1)S(1)}, bf16[2048,256]{1,0:T(8,128)(2,1)}, u32[]{:S(2)}) copy-start(bf16[2048,256]{1,0:T(8,128)(2,1)} %param.22) | copy-start | bytes 3145732
  71.8 6.1 %copy-start.7 = (bf16[16,2048]{1,0:T(8,128)(2,1)S(1)}, bf16[16,2048]{1,0:T(8,128)(2,1)}, u32[]{:S(2)}) copy-start(bf16[16,2048]{1,0:T(8,128)(2,1)} %param.14) | copy-start | bytes 196612
  73.2 19.8 %all-to-all-start.1 = ((bf16[8,32,2048]{2,1,0:T(8,128)(2,1)}), bf16[8,32,2048]{2,1,0:T(8,128)(2,1)S(1)}, u32[]{:S(2)}, u32[]{:S(2)}) async-start(bf16[8,32,2048]{2,1,0:T(8,128)(2,1)} %broadcast_in_dim.13), calls=%async_computation.1 | async-start | bytes 2097152 | tf_op jit(solution)/shard_map/all_to_all | solution.py:28
  78.0 69.1 %all-gather.2.cloned.1.call-start = ((), (), s32[]{:S(2)}) async-start(), calls=%async_computation.3 | async-start | bytes 1114112 | tf_op jit(solution)/shard_map/all_gather | solution.py:47
  92.9 1.2 copy-start.4
  92.9 4.3 %copy-start.6 = (bf16[2048,256]{1,0:T(8,128)(2,1)S(1)}, bf16[2048,256]{1,0:T(8,128)(2,1)}, u32[]{:S(2)}) copy-start(bf16[2048,256]{1,0:T(8,128)(2,1)} %param.21) | copy-start | bytes 3145732
  94.6 3.8 %collective-permute-start = (bf16[2,4,32,256]{3,2,0,1:T(8,128)(2,1)S(1)}, bf16[2,4,32,256]{3,2,0,1:T(8,128)(2,1)S(1)}, u32[]{:S(2)}, u32[]{:S(2)}) collective-permute-start(bf16[2,4,32,256]{3,2,0,1:T(8,128)(2,1)S(1)} %get-tuple-element.9), channel_id=1, source_target_pairs={{0,8},{8,16},{16,24},{24,32},{32,40},{40,48},{48,56},{56,64},{64,7... | collective-permute-start | bytes 393224 | tf_op jit(solution)/shard_map/ppermute | solution.py:59
  95.9 5.8 %collective-permute-start.1 = (bf16[2,4,32,256]{3,2,0,1:T(8,128)(2,1)S(1)}, bf16[2,4,32,256]{3,2,0,1:T(8,128)(2,1)}, u32[]{:S(2)}, u32[]{:S(2)}) collective-permute-start(bf16[2,4,32,256]{3,2,0,1:T(8,128)(2,1)S(1)} %get-tuple-element.10), channel_id=1, source_target_pairs={{8,0},{16,8},{24,16},{32,24},{40,32},{48,40},{56,48},{64,56},{72,6... | collective-permute-start | bytes 393224 | tf_op jit(solution)/shard_map/ppermute | solution.py:61
  98.4 0.7 copy-start.10
  107.9 4.5 %copy-start.1 = (f32[2,32,32,8,8]{1,2,4,0,3:T(8,128)S(1)}, f32[2,32,32,8,8]{1,2,4,0,3:T(8,128)}, u32[]{:S(2)}) copy-start(f32[2,32,32,8,8]{1,2,4,0,3:T(8,128)} %copy.76) | copy-start | bytes 1572868
  115.5 34.5 %copy-start.9 = (bf16[8,32,2,128]{3,1,0,2:T(8,128)(2,1)S(1)}, bf16[8,32,2,128]{3,1,0,2:T(8,128)(2,1)}, u32[]{:S(2)}) copy-start(bf16[8,32,2,128]{3,1,0,2:T(8,128)(2,1)} %copy.78) | copy-start | bytes 393220
  151.5 1.6 copy-start.2
  155.5 2.5 %copy-start.8 = (bf16[1024,2,128]{2,1,0:T(2,128)(2,1)S(1)}, bf16[1024,2,128]{2,1,0:T(2,128)(2,1)}, u32[]{:S(2)}) copy-start(bf16[1024,2,128]{2,1,0:T(2,128)(2,1)} %reshape_squeeze.15) | copy-start | bytes 1572868
Sparse Core Ops, SparseCore 0:
  90.0 56.9 all-gather.1
where the time goes:
time: 198 us; the launch traced here: 197 us
  blocking collectives  79.7 us (40%)
  waiting for transfers between devices  37.2 us (19%)
  local copies, waits for them, and re-layouts  22.5 us (11%)
  starting transfers between devices  21.4 us (11%)
  matrix products  16.3 us (8%)
  between operations  13.7 us (7%)
  other arithmetic  6.17 us (3%)
    psum x2, blocking collectives, one_axis_at_a_time(): array = lax.psum(array, axis)  39.6 us
    all_gather x1, waiting for transfers between devices, gathered_by_axis(): whole = lax.all_gather(whole, axes[number], axis=dim, tiled=True)  31.5 us
    all_to_all x1, blocking collectives, summed_on_arrival(): lax.all_to_all(parts, axis, split_axis=0, concat_axis=0, tiled=True)  30 us
    all_to_all x2, starting transfers between devices, sent_to_all(): lax.all_to_all(jnp.broadcast_to(array[None], (size, *array.shape)), axis,...  18.8 us
    all_gather x1, blocking collectives, gathered_by_axis(): whole = lax.all_gather(whole, axes[number], axis=dim, tiled=True)  10.1 us
  transfers between devices with their start and end apart: 5, of which 3 were waited for; matrix products, arithmetic and copies ran while one was open for 13% of the time, Pallas kernels for 0%

commit v1 on v0

v1 whole, which is shorter than its diff:
```python
import jax
import jax.numpy as jnp
from jax import lax
from jax.experimental import pallas as pl
from jax.experimental.pallas import tpu as pltpu
from jax.sharding import Mesh
from jax.sharding import PartitionSpec as P

HEADS = 16
HEAD_DIM = 128
GRID_W = 32
WIN_H = 8
WIN_W = 16
NORM_EPS = 1e-06
NEG_BIG = -1e30
NZ, NY, NX, NC = 16, 4, 4, 2
NSP = NZ * NY
GRID_R = 512
D = 2048
F32 = jnp.float32
BF16 = jnp.bfloat16
A_OFFS = (4, -3, 3, -2, 2, -1, 1)
B_OFFS = (4, -4)


def dot(a, b):
    return jnp.dot(a, b, preferred_element_type=F32)


def dot_t(a, b):
    return lax.dot_general(a, b, (((1,), (1,)), ((), ())), preferred_element_type=F32)


def silu(v):
    return v / (1.0 + jnp.exp(-v))


def kernel(
    lat_hbm, ctx_hbm, cond_hbm, cctx_hbm, gain_hbm, wsh_hbm, wsc_hbm, wga_hbm,
    wq_hbm, wk_hbm, wv_hbm, wo_hbm, rb_hbm, out_ref,
    latb, ctxb, condv, gainv, wmod, wq, wk, wv, wob, rbv,
    pbuf, abuf, sbuf, bbuf, tbuf, cbuf, mod,
    gmv, shv, gatev, rl, rc, xn, xc, qbuf, kbuf, vbuf, kvc, rolled, bias,
    att, attp, obuf, rbuf,
    ld, snd, a_r, b_r, c_r, m_r, lat_r, ring_r, part_r, wo_r, kv_r, att_r, out_r,
):
    z, y, x, c = (lax.axis_index(name) for name in ("z", "y", "x", "c"))
    t = x * 2 + c
    sp = z * NY + y
    pc = 1 - c
    sends = []

    def zz(d):
        return lax.rem(z + (NZ + d), NZ)

    def yy(d):
        return lax.rem(y + (NY + d), NY)

    def xx(d):
        return lax.rem(x + (NX + d), NX)

    def spd(d):
        other = lax.rem(sp + (NSP + d), NSP)
        return (other // NY, lax.rem(other, NY), x, c)

    def rcopy(src, dst, ssem, rsem, dev):
        return pltpu.make_async_remote_copy(
            src_ref=src, dst_ref=dst, send_sem=ssem, recv_sem=rsem,
            device_id=dev, device_id_type=pl.DeviceIdType.MESH,
        )

    def send(src, dst, rsem, dev):
        copy = rcopy(src, dst, snd.at[len(sends)], rsem, dev)
        copy.start()
        sends.append(copy)

    partner = (z, y, x, pc)

    def arrive(dst, rsem):
        rcopy(dst, dst, snd.at[0], rsem, partner).wait_recv()

    barrier = pltpu.get_barrier_semaphore()
    greet = [(zz(d), y, x, c) for d in (1, 2, 3, 4, -1, -2, -3, -4)]
    greet += [(z, yy(d), x, c) for d in (1, 2, 3)]
    greet += [
        (z, y, xx(dx), c if dc == 0 else pc) for dx in range(4) for dc in range(2) if dx or dc
    ]
    greet += [spd(1), spd(-1)]
    for dev in greet:
        pl.semaphore_signal(barrier, inc=1, device_id=dev, device_id_type=pl.DeviceIdType.MESH)

    wmod[...] = jnp.zeros_like(wmod)
    mine = pl.ds(pl.multiple_of(y * 32, 32), 32)
    loads = [
        (cond_hbm, condv.at[0]),
        (cctx_hbm, condv.at[1]),
        (wsh_hbm, wmod.at[0, mine, :]),
        (wsc_hbm, wmod.at[1, mine, :]),
        (wga_hbm, wmod.at[2, mine, :]),
        (lat_hbm, latb.at[4 + t]),
        (ctx_hbm.at[:, pl.ds(0, 1024)], ctxb.at[z, 0]),
        (ctx_hbm.at[:, pl.ds(1024, 1024)], ctxb.at[z, 1]),
        (rb_hbm.at[pl.ds(2 * t, 2)], rbv),
        (wo_hbm, wob.at[c]),
        (gain_hbm, gainv),
        (wk_hbm, wk),
        (wv_hbm, wv),
        (wq_hbm, wq),
    ]
    local = [pltpu.make_async_copy(s, d, ld.at[i]) for i, (s, d) in enumerate(loads)]
    for copy in local:
        copy.start()

    for i in range(5):
        local[i].wait()
    lane = lax.broadcasted_iota(jnp.int32, (8, 128), 1)
    row = lax.broadcasted_iota(jnp.int32, (8, 128), 0)
    keep = (lane >= y * 32) & (lane < y * 32 + 32)
    a0 = jnp.where(keep, silu(condv[0, pl.ds(z, 1), :]), 0.0)
    a1 = jnp.where(keep, silu(condv[1, pl.ds(z, 1), :]), 0.0)
    total = None
    for i in range(3):
        lhs = jnp.where(row == 2 * i, a0, 0.0)
        if i < 2:
            lhs = jnp.where(row == 2 * i + 1, a1, lhs)
        term = dot(lhs.astype(BF16), wmod[i])
        total = term if total is None else total + term
    pbuf[0:8, :] = total[:, :128]
    pbuf[8:16, :] = total[:, 128:]
    for i in range(5, 8):
        local[i].wait()
    pl.semaphore_wait(barrier, len(greet))

    for k, d in enumerate(A_OFFS):
        send(pbuf, abuf.at[k], a_r.at[k], (zz(d), y, x, c))

    def ring(slot, d):
        send(ctxb.at[slot, c], ctxb.at[slot, c], ring_r.at[slot], (zz(d), y, x, c))

    def to_partner_ctx(slot):
        send(ctxb.at[slot, c], ctxb.at[slot, c], part_r.at[slot], partner)

    def lat_send(slot, dev):
        send(latb.at[slot], latb.at[slot], lat_r.at[slot], dev)

    own_slot = 4 + t
    halo_slot = lax.rem(t + 12, 16)
    for d in (2, -2, 1, -1):
        ring(z, d)
    to_prev = x < 2
    spn = lax.rem(sp + jnp.where(to_prev, NSP - 1, 1), NSP)
    send(
        latb.at[own_slot], latb.at[halo_slot], lat_r.at[halo_slot],
        (spn // NY, lax.rem(spn, NY), x, c),
    )

    def lat_out(slot):
        for dx in (2, 1, 3):
            lat_send(slot, (z, y, xx(dx), c))
        lat_send(slot, partner)

    lat_out(own_slot)

    def ring_in(d):
        slot = zz(-d)
        arrive(ctxb.at[slot, c], ring_r.at[slot])
        return slot

    def ring_step(d):
        for sign in (1, -1):
            if sign == -1 and d == 8:
                continue
            slot = ring_in(sign * d)
            if d in (2, 4, 6):
                if not (sign == -1 and d == 6):
                    ring(slot, 2 * sign)
                ring(slot, sign)
            to_partner_ctx(slot)

    local[8].wait()
    row32 = lax.broadcasted_iota(jnp.int32, (32, 128), 0)
    lane32 = lax.broadcasted_iota(jnp.int32, (32, 128), 1)
    c2 = lax.rem(lane32, 32)
    b0 = jnp.clip(row32 - WIN_W // 2, 0, GRID_W - WIN_W)
    col_in = (c2 >= b0) & (c2 < b0 + WIN_W)
    quarter = lane32 // 32

    def bias_head(h, carry):
        def roll_e(e, inner):
            line = jnp.broadcast_to(rbv[h, pl.ds(e, 1), :], (32, 128))
            for k in range(4):
                rolled[e, k] = pltpu.roll(line, (32 * k + 113) % 128, 1, stride=1, stride_axis=0)
            return inner

        lax.fori_loop(0, 15, roll_e, 0)
        for i in range(8):
            first = sp * 8
            start = jnp.clip(first + i - WIN_H // 2, 0, GRID_R - WIN_H) - first + 4
            for q in range(4):
                tile = jnp.full((32, 128), NEG_BIG, F32)
                for k in range(4):
                    e = 4 * q + k - i + 3
                    if 0 <= e < 15:
                        tile = jnp.where(quarter == k, rolled[e, k], tile)
                j = 4 * q + quarter
                ok = col_in & (j >= start) & (j < start + WIN_H)
                bias[h, i % 2, (i // 2) * 32 : (i // 2) * 32 + 32, q * 128 : q * 128 + 128] = (
                    jnp.where(ok, tile, NEG_BIG)
                )
        return carry

    lax.fori_loop(0, 2, bias_head, 0)

    ring_step(1)
    ring_step(2)

    for k in range(7):
        arrive(abuf.at[k], a_r.at[k])
    part = pbuf[...]
    for k in range(7):
        part = part + abuf[k]
    sbuf[...] = part
    for k, d in enumerate(B_OFFS):
        send(sbuf, bbuf.at[k], b_r.at[k], (zz(d), y, x, c))

    arrive(latb.at[halo_slot], lat_r.at[halo_slot])
    lat_out(halo_slot)
    local[9].wait()
    send(wob.at[c], wob.at[c], wo_r, partner)

    ring_step(3)
    ring_step(4)

    for k in range(2):
        arrive(bbuf.at[k], b_r.at[k])
    tbuf[...] = bbuf[0] + bbuf[1]
    for k in range(3):
        send(tbuf, cbuf.at[k], c_r.at[k], (z, yy(k + 1), x, c))

    def lat_in(slot):
        arrive(latb.at[slot], lat_r.at[slot])

    for dx in (1, 3, 2):
        slot = 4 + xx(dx) * 2 + c
        lat_in(slot)
        lat_send(slot, partner)
    ring_step(5)
    ring_step(6)

    for k in range(3):
        arrive(cbuf.at[k], c_r.at[k])
    mod[t] = tbuf[...] + cbuf[0] + cbuf[1] + cbuf[2]
    for dx in (2, 1, 3, 0):
        for dc in range(2):
            if dx or dc:
                send(mod.at[t], mod.at[t], m_r.at[t], (z, y, xx(dx), c if dc == 0 else pc))

    for dx in (1, 3, 2):
        slot = lax.rem(xx(dx) * 2 + c + 12, 16)
        lat_in(slot)
        lat_send(slot, partner)
    ring_step(7)
    ring_step(8)

    for d in range(1, NZ):
        slot = zz(d)
        arrive(ctxb.at[slot, pc], part_r.at[slot])
    for dx in range(4):
        other = xx(dx) * 2 + pc
        lat_in(4 + other)
        lat_in(lax.rem(other + 12, 16))

    def ctx_tile(g, j):
        block = ctxb[pl.ds(8 * g, 8), j // 8, :, (j % 8) * 128 : (j % 8) * 128 + 128]
        return block.reshape(128, 128).astype(F32)

    def lat_tile(g, j):
        return latb[pl.ds(4 * g, 4), :, j * 128 : j * 128 + 128].reshape(128, 128).astype(F32)

    def stats(tile_of, dest, count):
        def step(g, carry):
            acc = jnp.zeros((128, 128), F32)
            for j in range(16):
                tile = tile_of(g, j)
                acc = acc + tile * tile
            mean = jnp.sum(acc, axis=1, keepdims=True) * (1.0 / D)
            dest[pl.ds(pl.multiple_of(128 * g, 128), 128), :] = jnp.broadcast_to(
                lax.rsqrt(mean + NORM_EPS), (128, 128)
            )
            return carry

        lax.fori_loop(0, count, step, 0)

    stats(ctx_tile, rc, 2)
    stats(lat_tile, rl, 4)
    local[10].wait()
    for dx in range(4):
        for dc in range(2):
            if dx or dc:
                slot = xx(dx) * 2 + (c if dc == 0 else pc)
                arrive(mod.at[slot], m_r.at[slot])
    for j in range(16):
        low = (j % 2) * 8
        for which in range(2):
            gmv[which, j : j + 1, :] = gainv[j : j + 1, :] * (
                1.0 + mod[j // 2, low + 2 + which : low + 3 + which, :]
            )
            shv[which, j : j + 1, :] = mod[j // 2, low + which : low + which + 1, :]
        gatev[j : j + 1, :] = mod[j // 2, low + 4 : low + 5, :]

    def normed(tile_of, scale, which, dest, count):
        def step(g, carry):
            rows = pl.ds(pl.multiple_of(128 * g, 128), 128)
            inv = scale[rows, :]
            for j in range(16):
                value = tile_of(g, j) * inv * gmv[which, j : j + 1, :] + shv[which, j : j + 1, :]
                dest[rows, j * 128 : j * 128 + 128] = value.astype(BF16)
            return carry

        lax.fori_loop(0, count, step, 0)

    normed(ctx_tile, rc, 1, xc, 2)
    local[11].wait()
    local[12].wait()
    kvc[y, :, 0:256] = dot(xc[...], wk[...]).astype(BF16)
    kvc[y, :, 256:512] = dot(xc[...], wv[...]).astype(BF16)

    def kv_send(slot, half, d, k):
        ref = kvc.at[slot, pl.ds(128 * half, 128), :]
        send(ref, ref, kv_r.at[k], (z, yy(d), x, c))

    def kv_in(d, half, k):
        arrive(kvc.at[yy(d), pl.ds(128 * half, 128), :], kv_r.at[k])

    kv_send(y, 0, 1, 0)
    kv_send(y, 1, -1, 1)
    kv_send(y, 1, 1, 2)
    kv_send(y, 0, -1, 3)

    normed(lat_tile, rl, 0, xn, 4)
    kv_in(-1, 0, 0)
    kv_send(yy(-1), 0, 1, 4)
    kv_in(1, 1, 1)
    kv_send(yy(1), 1, -1, 5)

    def project(g, carry):
        rows = pl.ds(pl.multiple_of(256 * g, 256), 256)
        kbuf[rows, :] = dot(xn[rows, :], wk[...]).astype(BF16)
        vbuf[rows, :] = dot(xn[rows, :], wv[...]).astype(BF16)
        return carry

    lax.fori_loop(0, 2, project, 0)
    local[13].wait()
    queries = dot(xn[128:384, :], wq[...]).astype(BF16)
    for i in range(8):
        qbuf[i % 2, (i // 2) * 32 : (i // 2) * 32 + 32, :] = queries[i * 32 : i * 32 + 32, :]

    kv_in(-1, 1, 2)
    kv_in(1, 0, 3)
    kv_in(2, 0, 4)
    kv_in(2, 1, 5)

    inv_scale = HEAD_DIM**-0.5

    def attend(par):
        for h in range(2):
            cols = slice(h * 128, h * 128 + 128)
            vcols = slice(256 + h * 128, 256 + h * 128 + 128)
            q = qbuf[par, :, cols]
            s_win = dot_t(q, kbuf[:, cols]) * inv_scale + bias[h, par]
            s_ctx = dot_t(q, kvc[:, :, cols].reshape(1024, 128)) * inv_scale
            top = jnp.maximum(
                jnp.max(s_win, axis=1, keepdims=True), jnp.max(s_ctx, axis=1, keepdims=True)
            )
            e_win = jnp.exp(s_win - top)
            e_ctx = jnp.exp(s_ctx - top)
            norm = jnp.sum(e_win, axis=1, keepdims=True) + jnp.sum(e_ctx, axis=1, keepdims=True)
            mixed = dot(e_win.astype(BF16), vbuf[:, cols]) + dot(
                e_ctx.astype(BF16), kvc[:, :, vcols].reshape(1024, 128)
            )
            att[par, :, cols] = (mixed / norm).astype(BF16)

    attend(pc)
    send(att.at[pc], attp, att_r, partner)
    attend(c)
    arrive(attp, att_r)
    arrive(wob.at[pc], wo_r)

    def out_cols(n, carry):
        cols = pl.ds(pl.multiple_of(512 * n, 512), 512)
        value = dot(att[c], wob[c, :, cols]) + dot(attp[...], wob[pc, :, cols])
        obuf[:, :, cols] = value.astype(BF16).reshape(4, 32, 512)
        return carry

    lax.fori_loop(0, 4, out_cols, 0)
    for dx in (2, 1, 3):
        send(obuf.at[xx(dx)], rbuf.at[dx - 1], out_r.at[dx - 1], (z, y, xx(dx), c))
    for dx in (1, 3, 2):
        arrive(rbuf.at[dx - 1], out_r.at[dx - 1])
    for j in range(16):
        cols = slice(j * 128, j * 128 + 128)
        branch = obuf[x, :, cols].astype(F32)
        for k in range(3):
            branch = branch + rbuf[k, :, cols].astype(F32)
        out_ref[:, cols] = (
            latb[own_slot, :, cols].astype(F32) + gatev[j : j + 1, :] * branch
        ).astype(BF16)
    for copy in sends:
        copy.wait_send()


N_SENDS = 7 + 4 + 1 + 4 + 11 + 15 + 2 + 4 + 1 + 3 + 3 + 7 + 3 + 6 + 1 + 3


def on_device(
    latent, context, condition, ctx_cond, norm_gain, w_shift, w_scale, w_gate,
    w_query, w_key, w_value, w_out, rel_bias,
):
    vm = pltpu.VMEM
    dma = pltpu.SemaphoreType.DMA
    bias_rows = jnp.pad(rel_bias, ((0, 0), (0, 1), (0, 97)))
    return pl.pallas_call(
        kernel,
        out_shape=jax.ShapeDtypeStruct((32, D), BF16),
        in_specs=[pl.BlockSpec(memory_space=pl.ANY)] * 13,
        out_specs=pl.BlockSpec(memory_space=pltpu.VMEM),
        scratch_shapes=[
            vm((16, 32, D), BF16),
            vm((16, 2, 16, 1024), BF16),
            vm((2, 16, 128), F32),
            vm((16, 128), F32),
            vm((3, 128, 256), BF16),
            vm((D, 256), BF16),
            vm((D, 256), BF16),
            vm((D, 256), BF16),
            vm((2, 256, D), BF16),
            vm((2, 16, 128), F32),
            vm((16, 128), F32),
            vm((7, 16, 128), F32),
            vm((16, 128), F32),
            vm((2, 16, 128), F32),
            vm((16, 128), F32),
            vm((3, 16, 128), F32),
            vm((8, 16, 128), F32),
            vm((2, 16, 128), F32),
            vm((2, 16, 128), F32),
            vm((16, 128), F32),
            vm((512, 128), F32),
            vm((256, 128), F32),
            vm((512, D), BF16),
            vm((256, D), BF16),
            vm((2, 128, 256), BF16),
            vm((512, 256), BF16),
            vm((512, 256), BF16),
            vm((4, 256, 512), BF16),
            vm((15, 4, 32, 128), F32),
            vm((2, 2, 128, 512), F32),
            vm((2, 128, 256), BF16),
            vm((128, 256), BF16),
            vm((4, 32, D), BF16),
            vm((3, 32, D), BF16),
            dma((14,)),
            dma((N_SENDS,)),
            dma((7,)),
            dma((2,)),
            dma((3,)),
            dma((8,)),
            dma((16,)),
            dma((16,)),
            dma((16,)),
            dma(()),
            dma((6,)),
            dma(()),
            dma((3,)),
        ],
        compiler_params=pltpu.CompilerParams(
            collective_id=0, has_side_effects=True, vmem_limit_bytes=56 * 1024 * 1024
        ),
        name="whole_step",
    )(
        latent, context, condition.reshape(16, 128), ctx_cond.reshape(16, 128),
        norm_gain.reshape(16, 128), w_shift, w_scale, w_gate, w_query, w_key, w_value, w_out,
        bias_rows,
    )


def solution(mesh):
    torus = Mesh(mesh.devices.reshape(NZ, NY, NX, NC), ("z", "y", "x", "c"))
    sp, tp = ("z", "y"), ("x", "c")
    return jax.shard_map(
        on_device,
        mesh=torus,
        in_specs=(
            P((*sp, *tp), None),
            P(sp, None),
            P(),
            P(),
            P(),
            P(sp, tp),
            P(sp, tp),
            P(sp, tp),
            P(None, tp),
            P(None, tp),
            P(None, tp),
            P(tp, None),
            P(),
        ),
        out_specs=P((*sp, *tp), None),
        check_vma=False,
    )
```

time: 198 us -> 65.5 us (0.33)
  blocking collectives: 79.7 us -> 0 us
  Pallas kernels: 0 us -> 62.2 us
  waiting for transfers between devices: 37.2 us -> 0 us
  starting transfers between devices: 21.4 us -> 0 us
  local copies, waits for them, and re-layouts: 22.5 us -> 3.18 us
  matrix products: 16.3 us -> 0 us
  between operations: 13.7 us -> 0.01 us
  other arithmetic: 6.17 us -> 0 us
    pallas_call x0 -> x1, Pallas kernels: none -> 62.2 us  [on_device(): pl.pallas_call(kernel, out_shape=jax.ShapeDtypeStruct((32, D), BF16), in_...]
    psum x2 -> x0, blocking collectives: 39.6 us -> none  [one_axis_at_a_time(): array = lax.psum(array, axis)]
    all_gather x1 -> x0, waiting for transfers between devices: 31.5 us -> none  [gathered_by_axis(): whole = lax.all_gather(whole, axes[number], axis=dim, tiled=True)]
    all_to_all x1 -> x0, blocking collectives: 30 us -> none  [summed_on_arrival(): lax.all_to_all(parts, axis, split_axis=0, concat_axis=0, tiled=True)]
    all_to_all x2 -> x0, starting transfers between devices: 18.8 us -> none  [sent_to_all(): lax.all_to_all(jnp.broadcast_to(array[None], (size, *array.shape)), axis,...]
    dot_general x14 -> x0, matrix products: 14.8 us -> none  [the longest x1 3.15 us: on_device(): jnp.einsum('rqhd,rkwhd->rqhkw', queries, key_win, preferred_element_type=...]
    all_gather x1 -> x0, blocking collectives: 10.1 us -> none  [gathered_by_axis(): whole = lax.all_gather(whole, axes[number], axis=dim, tiled=True)]
    another operation x6 -> x0, local copies, waits for them, and re-layouts: 8.11 us -> none  [the longest x1 2.3 us: on_device(): windows[:, 0].reshape(grid_rows, WIN_H, GRID_W, head_dev, HEAD_DIM)]
  transfers between devices with their start and end apart: 5 -> 0, of which waited for: 3 -> 0; matrix products, arithmetic and copies ran while one was open for 13% -> 0% of each run, Pallas kernels for 0% -> 0%
where the time goes in v1:
time: 65.5 us; the launch traced here: 65.4 us
  Pallas kernels  62.2 us (95%)
  local copies, waits for them, and re-layouts  3.18 us (5%)
    pallas_call x1, Pallas kernels, on_device(): pl.pallas_call(kernel, out_shape=jax.ShapeDtypeStruct((32, D), BF16), in_...  62.2 us
    unnamed x2, local copies, waits for them, and re-layouts  2.51 us

profile of v1, /device:TPU:1, one launch (start us, length us, event | category | flops | bytes accessed | tf_op | source)
XLA Modules:
  0.0 65.4 jit_solution(12622123206792585137)
XLA Ops:
  0.0 0.9 %copy.14 = f32[16,15,31]{2,1,0:T(8,128)S(1)} copy(f32[16,15,31]{2,0,1:T(8,128)} %param.25) | data formatting | bytes 59520 | tf_op args[12]
  0.9 0.7 %pad.4.rb_hbm = f32[16,16,128]{2,1,0:T(8,128)} pad(f32[16,15,31]{2,1,0:T(8,128)S(1)} %copy.14, f32[]{:T(128)} %constant.2.clone.1), padding=0_0x0_1x0_97 | pad | bytes 160836 | tf_op jit(solution)/shard_map/jit(_pad)/pad | solution.py:421
  1.6 62.2 %whole_step.1 = bf16[32,2048]{1,0:T(8,128)(2,1)} custom-call(bf16[32,2048]{1,0:T(8,128)(2,1)} %lat_hbm.1, bf16[16,2048]{1,0:T(8,128)(2,1)} %ctx_hbm.1, f32[16,128]{1,0:T(8,128)} %bitcast.3, f32[16,128]{1,0:T(8,128)} %bitcast.4, f32[16,128]{1,0:T(8,128)} %bitcast.5, bf16[32,256]{1,0:T(8,128)(2,1)} %wsh_hbm.1, bf16[32,256]{1,0:T(8,128)(2,1)} %wsc_hbm.1, ...), custom_call_target="tpu_custom_call" | custom-call | tf_op jit(solution)/shard_map/whole_step/pallas_call | solution.py:422
  63.8 1.6 %copy.16 = bf16[32,2048]{1,0:T(8,128)(2,1)} copy(bf16[32,2048]{1,0:T(8,128)(2,1)} %whole_step.1) | data formatting | bytes 262144

commit v2 on v1

--- a/solution.py
+++ b/solution.py
@@ -21,6 +21,7 @@
 BF16 = jnp.bfloat16
 A_OFFS = (4, -3, 3, -2, 2, -1, 1)
 B_OFFS = (4, -4)
+GROUPS = ((0, 1), (1, 5), (5, 9), (9, 13), (13, 16))
 
 
 def dot(a, b):
@@ -42,7 +43,8 @@
     pbuf, abuf, sbuf, bbuf, tbuf, cbuf, mod,
     gmv, shv, gatev, rl, rc, xn, xc, qbuf, kbuf, vbuf, kvc, rolled, bias,
     att, attp, obuf, rbuf,
-    ld, snd, a_r, b_r, c_r, m_r, lat_r, ring_r, part_r, wo_r, kv_r, att_r, out_r,
+    ld, snd, a_r, b_r, c_r, m_r, lat_r, ring_r, own_r, y_r, y_p, far_r, far_p,
+    wo_r, att_r, out_r,
 ):
     z, y, x, c = (lax.axis_index(name) for name in ("z", "y", "x", "c"))
     t = x * 2 + c
@@ -79,6 +81,16 @@
     def arrive(dst, rsem):
         rcopy(dst, dst, snd.at[0], rsem, partner).wait_recv()
 
+    scope = []
+
+    def phase(name):
+        if scope:
+            scope.pop().__exit__(None, None, None)
+        if name:
+            scope.append(jax.named_scope(name))
+            scope[0].__enter__()
+
+    phase("greet")
     barrier = pltpu.get_barrier_semaphore()
     greet = [(zz(d), y, x, c) for d in (1, 2, 3, 4, -1, -2, -3, -4)]
     greet += [(z, yy(d), x, c) for d in (1, 2, 3)]
@@ -98,8 +110,8 @@
         (wsc_hbm, wmod.at[1, mine, :]),
         (wga_hbm, wmod.at[2, mine, :]),
         (lat_hbm, latb.at[4 + t]),
-        (ctx_hbm.at[:, pl.ds(0, 1024)], ctxb.at[z, 0]),
-        (ctx_hbm.at[:, pl.ds(1024, 1024)], ctxb.at[z, 1]),
+        (ctx_hbm.at[:, pl.ds(0, 1024)], ctxb.at[0, 0, 0]),
+        (ctx_hbm.at[:, pl.ds(1024, 1024)], ctxb.at[0, 1, 0]),
         (rb_hbm.at[pl.ds(2 * t, 2)], rbv),
         (wo_hbm, wob.at[c]),
         (gain_hbm, gainv),
@@ -111,8 +123,10 @@
     for copy in local:
         copy.start()
 
+    phase("mod_load")
     for i in range(5):
         local[i].wait()
+    phase("mod_term")
     lane = lax.broadcasted_iota(jnp.int32, (8, 128), 1)
     row = lax.broadcasted_iota(jnp.int32, (8, 128), 0)
     keep = (lane >= y * 32) & (lane < y * 32 + 32)
@@ -127,26 +141,101 @@
         total = term if total is None else total + term
     pbuf[0:8, :] = total[:, :128]
     pbuf[8:16, :] = total[:, 128:]
+    phase("wait_barrier")
     for i in range(5, 8):
         local[i].wait()
     pl.semaphore_wait(barrier, len(greet))
 
-    for k, d in enumerate(A_OFFS):
-        send(pbuf, abuf.at[k], a_r.at[k], (zz(d), y, x, c))
-
-    def ring(slot, d):
-        send(ctxb.at[slot, c], ctxb.at[slot, c], ring_r.at[slot], (zz(d), y, x, c))
-
-    def to_partner_ctx(slot):
-        send(ctxb.at[slot, c], ctxb.at[slot, c], part_r.at[slot], partner)
+    phase("send_first")
+    for k in range(3):
+        send(pbuf, cbuf.at[k], c_r.at[k], (z, yy(k + 1), x, c))
+
+    def piece(r, half, lo, hi):
+        return ctxb.at[r, half, pl.ds(lo, hi - lo)]
+
+    def ring(slot, sub, d):
+        near = (slot + 1) // 2
+        far = near + abs(d)
+        to = 2 * far - 1 if d > 0 else 2 * far
+        cols = pl.ds(512 * sub, 512)
+        send(
+            ctxb.at[0, c, slot, :, cols], ctxb.at[0, c, to, :, cols],
+            ring_r.at[to, sub], (zz(d), y, x, c),
+        )
+
+    def ring_group(g):
+        lo, hi = GROUPS[g]
+        for sub in range(2):
+            cols = pl.ds(512 * sub, 512)
+            for slot in sorted(range(lo, hi), key=lambda s: ((s + 1) // 2) % 2):
+                arrive(ctxb.at[0, c, slot, :, cols], ring_r.at[slot, sub])
+                near, sign = (slot + 1) // 2, 1 if slot % 2 else -1
+                if near in (2, 4, 6):
+                    if not (sign == -1 and near == 6):
+                        ring(slot, sub, 2 * sign)
+                    ring(slot, sub, sign)
+        y_out(g)
+        own = piece(0, c, lo, hi)
+        send(own, own, own_r.at[g], partner)
+
+    def y_out(g):
+        lo, hi = GROUPS[g]
+        for k in range(2):
+            send(
+                piece(0, c, lo, hi), piece(1 + k, c, lo, hi), y_r.at[k, g],
+                (z, yy(1 if k == 0 else -1), x, c),
+            )
+
+    def halves(g):
+        lo, hi = GROUPS[g]
+        mid = (lo + hi + (g == 0)) // 2
+        return ((lo, mid), (mid, hi))
+
+    def y_in(g):
+        lo, hi = GROUPS[g]
+        for k in range(2):
+            got = piece(1 + k, c, lo, hi)
+            arrive(got, y_r.at[k, g])
+            first, last = halves(g)[k]
+            if last > first:
+                send(
+                    piece(1 + k, c, first, last), piece(3, c, first, last), far_r.at[k, g],
+                    (z, yy(1 if k == 0 else -1), x, c),
+                )
+            send(got, got, y_p.at[k, g], partner)
+
+    def far_in(g):
+        for k in range(2):
+            first, last = halves(g)[k]
+            if last > first:
+                got = piece(3, c, first, last)
+                arrive(got, far_r.at[k, g])
+                send(got, got, far_p.at[k, g], partner)
+
+    def own_ready():
+        for g in range(1, 5):
+            arrive(piece(0, pc, *GROUPS[g]), own_r.at[g])
+
+    def y_ready(k):
+        for g in range(5):
+            arrive(piece(1 + k, pc, *GROUPS[g]), y_p.at[k, g])
+
+    def far_ready():
+        for g in range(5):
+            for k in range(2):
+                first, last = halves(g)[k]
+                if last > first:
+                    arrive(piece(3, pc, first, last), far_p.at[k, g])
 
     def lat_send(slot, dev):
         send(latb.at[slot], latb.at[slot], lat_r.at[slot], dev)
 
     own_slot = 4 + t
     halo_slot = lax.rem(t + 12, 16)
-    for d in (2, -2, 1, -1):
-        ring(z, d)
+    for sub in range(2):
+        for d in (2, -2, 1, -1):
+            ring(0, sub, d)
+    y_out(0)
     to_prev = x < 2
     spn = lax.rem(sp + jnp.where(to_prev, NSP - 1, 1), NSP)
     send(
@@ -161,22 +250,7 @@
 
     lat_out(own_slot)
 
-    def ring_in(d):
-        slot = zz(-d)
-        arrive(ctxb.at[slot, c], ring_r.at[slot])
-        return slot
-
-    def ring_step(d):
-        for sign in (1, -1):
-            if sign == -1 and d == 8:
-                continue
-            slot = ring_in(sign * d)
-            if d in (2, 4, 6):
-                if not (sign == -1 and d == 6):
-                    ring(slot, 2 * sign)
-                ring(slot, sign)
-            to_partner_ctx(slot)
-
+    phase("bias")
     local[8].wait()
     row32 = lax.broadcasted_iota(jnp.int32, (32, 128), 0)
     lane32 = lax.broadcasted_iota(jnp.int32, (32, 128), 1)
@@ -204,80 +278,90 @@
                         tile = jnp.where(quarter == k, rolled[e, k], tile)
                 j = 4 * q + quarter
                 ok = col_in & (j >= start) & (j < start + WIN_H)
-                bias[h, i % 2, (i // 2) * 32 : (i // 2) * 32 + 32, q * 128 : q * 128 + 128] = (
+                bias[h, i // 2, (i % 2) * 32 : (i % 2) * 32 + 32, q * 128 : q * 128 + 128] = (
                     jnp.where(ok, tile, NEG_BIG)
                 )
         return carry
 
     lax.fori_loop(0, 2, bias_head, 0)
 
-    ring_step(1)
-    ring_step(2)
-
-    for k in range(7):
-        arrive(abuf.at[k], a_r.at[k])
-    part = pbuf[...]
-    for k in range(7):
-        part = part + abuf[k]
-    sbuf[...] = part
-    for k, d in enumerate(B_OFFS):
-        send(sbuf, bbuf.at[k], b_r.at[k], (zz(d), y, x, c))
-
-    arrive(latb.at[halo_slot], lat_r.at[halo_slot])
+    def lat_in(slot):
+        arrive(latb.at[slot], lat_r.at[slot])
+
+    phase("mod_y")
+    for k in range(3):
+        arrive(cbuf.at[k], c_r.at[k])
+    sbuf[...] = (pbuf[...] + cbuf[0] + cbuf[1] + cbuf[2]).astype(BF16)
+    for k, d in enumerate(A_OFFS):
+        send(sbuf, abuf.at[k], a_r.at[k], (zz(d), y, x, c))
+
+    phase("ring1")
+    ring_group(1)
+    phase("halo")
+    lat_in(halo_slot)
     lat_out(halo_slot)
     local[9].wait()
     send(wob.at[c], wob.at[c], wo_r, partner)
-
-    ring_step(3)
-    ring_step(4)
-
-    for k in range(2):
-        arrive(bbuf.at[k], b_r.at[k])
-    tbuf[...] = bbuf[0] + bbuf[1]
-    for k in range(3):
-        send(tbuf, cbuf.at[k], c_r.at[k], (z, yy(k + 1), x, c))
-
-    def lat_in(slot):
-        arrive(latb.at[slot], lat_r.at[slot])
-
+    phase("y0")
+    y_in(0)
+
+    phase("mod_a")
+    for k in range(7):
+        arrive(abuf.at[k], a_r.at[k])
+    part = sbuf[...].astype(F32)
+    for k in range(7):
+        part = part + abuf[k].astype(F32)
+    tbuf[...] = part
+    for k, d in enumerate(B_OFFS):
+        send(tbuf, bbuf.at[k], b_r.at[k], (zz(d), y, x, c))
+
+    phase("lat_own")
     for dx in (1, 3, 2):
         slot = 4 + xx(dx) * 2 + c
         lat_in(slot)
         lat_send(slot, partner)
-    ring_step(5)
-    ring_step(6)
-
-    for k in range(3):
-        arrive(cbuf.at[k], c_r.at[k])
-    mod[t] = tbuf[...] + cbuf[0] + cbuf[1] + cbuf[2]
+    phase("ring2")
+    ring_group(2)
+    phase("y1")
+    y_in(1)
+    far_in(0)
+
+    phase("mod_b")
+    for k in range(2):
+        arrive(bbuf.at[k], b_r.at[k])
+    mod[t] = bbuf[0] + bbuf[1]
     for dx in (2, 1, 3, 0):
         for dc in range(2):
             if dx or dc:
                 send(mod.at[t], mod.at[t], m_r.at[t], (z, y, xx(dx), c if dc == 0 else pc))
 
+    phase("ring3")
+    ring_group(3)
+    phase("lat_halo")
     for dx in (1, 3, 2):
         slot = lax.rem(xx(dx) * 2 + c + 12, 16)
         lat_in(slot)
         lat_send(slot, partner)
-    ring_step(7)
-    ring_step(8)
-
-    for d in range(1, NZ):
-        slot = zz(d)
-        arrive(ctxb.at[slot, pc], part_r.at[slot])
+    phase("y2")
+    y_in(2)
+    far_in(1)
+
+    phase("lat_parts")
     for dx in range(4):
         other = xx(dx) * 2 + pc
         lat_in(4 + other)
         lat_in(lax.rem(other + 12, 16))
 
     def ctx_tile(g, j):
-        block = ctxb[pl.ds(8 * g, 8), j // 8, :, (j % 8) * 128 : (j % 8) * 128 + 128]
+        block = ctxb[
+            g // 2, j // 8, pl.ds(8 * lax.rem(g, 2), 8), :, (j % 8) * 128 : (j % 8) * 128 + 128
+        ]
         return block.reshape(128, 128).astype(F32)
 
     def lat_tile(g, j):
         return latb[pl.ds(4 * g, 4), :, j * 128 : j * 128 + 128].reshape(128, 128).astype(F32)
 
-    def stats(tile_of, dest, count):
+    def stats(tile_of, dest, first, count):
         def step(g, carry):
             acc = jnp.zeros((128, 128), F32)
             for j in range(16):
@@ -289,16 +373,20 @@
             )
             return carry
 
-        lax.fori_loop(0, count, step, 0)
-
-    stats(ctx_tile, rc, 2)
-    stats(lat_tile, rl, 4)
+        lax.fori_loop(first, first + count, step, 0)
+
+    phase("lat_stats")
+    stats(lat_tile, rl, 0, 4)
+    phase("ring4")
+    ring_group(4)
+    phase("mod_gather")
     local[10].wait()
     for dx in range(4):
         for dc in range(2):
             if dx or dc:
                 slot = xx(dx) * 2 + (c if dc == 0 else pc)
                 arrive(mod.at[slot], m_r.at[slot])
+    phase("mod_rows")
     for j in range(16):
         low = (j % 2) * 8
         for which in range(2):
@@ -308,40 +396,17 @@
             shv[which, j : j + 1, :] = mod[j // 2, low + which : low + which + 1, :]
         gatev[j : j + 1, :] = mod[j // 2, low + 4 : low + 5, :]
 
-    def normed(tile_of, scale, which, dest, count):
+    def normed(tile_of, scale, which, dest, first, count):
         def step(g, carry):
             rows = pl.ds(pl.multiple_of(128 * g, 128), 128)
+            to = pl.ds(pl.multiple_of(128 * (g - first), 128), 128)
             inv = scale[rows, :]
             for j in range(16):
                 value = tile_of(g, j) * inv * gmv[which, j : j + 1, :] + shv[which, j : j + 1, :]
-                dest[rows, j * 128 : j * 128 + 128] = value.astype(BF16)
+                dest[to, j * 128 : j * 128 + 128] = value.astype(BF16)
             return carry
 
-        lax.fori_loop(0, count, step, 0)
-
-    normed(ctx_tile, rc, 1, xc, 2)
-    local[11].wait()
-    local[12].wait()
-    kvc[y, :, 0:256] = dot(xc[...], wk[...]).astype(BF16)
-    kvc[y, :, 256:512] = dot(xc[...], wv[...]).astype(BF16)
-
-    def kv_send(slot, half, d, k):
-        ref = kvc.at[slot, pl.ds(128 * half, 128), :]
-        send(ref, ref, kv_r.at[k], (z, yy(d), x, c))
-
-    def kv_in(d, half, k):
-        arrive(kvc.at[yy(d), pl.ds(128 * half, 128), :], kv_r.at[k])
-
-    kv_send(y, 0, 1, 0)
-    kv_send(y, 1, -1, 1)
-    kv_send(y, 1, 1, 2)
-    kv_send(y, 0, -1, 3)
-
-    normed(lat_tile, rl, 0, xn, 4)
-    kv_in(-1, 0, 0)
-    kv_send(yy(-1), 0, 1, 4)
-    kv_in(1, 1, 1)
-    kv_send(yy(1), 1, -1, 5)
+        lax.fori_loop(first, first + count, step, 0)
 
     def project(g, carry):
         rows = pl.ds(pl.multiple_of(256 * g, 256), 256)
@@ -349,25 +414,57 @@
         vbuf[rows, :] = dot(xn[rows, :], wv[...]).astype(BF16)
         return carry
 
+    def context(r):
+        stats(ctx_tile, rc, 2 * r, 2)
+        normed(ctx_tile, rc, 1, xc, 2 * r, 2)
+        kvc[r, :, 0:256] = dot(xc[...], wk[...]).astype(BF16)
+        kvc[r, :, 256:512] = dot(xc[...], wv[...]).astype(BF16)
+
+    phase("y3")
+    y_in(3)
+    far_in(2)
+    for i in (11, 12, 13):
+        local[i].wait()
+    phase("lat_norm")
+    normed(lat_tile, rl, 0, xn, 0, 4)
+    phase("lat_proj")
     lax.fori_loop(0, 2, project, 0)
-    local[13].wait()
+    phase("lat_q")
     queries = dot(xn[128:384, :], wq[...]).astype(BF16)
     for i in range(8):
-        qbuf[i % 2, (i // 2) * 32 : (i // 2) * 32 + 32, :] = queries[i * 32 : i * 32 + 32, :]
-
-    kv_in(-1, 1, 2)
-    kv_in(1, 0, 3)
-    kv_in(2, 0, 4)
-    kv_in(2, 1, 5)
+        qbuf[i // 2, (i % 2) * 32 : (i % 2) * 32 + 32, :] = queries[i * 32 : i * 32 + 32, :]
+    phase("own_wait")
+    own_ready()
+    phase("ctx0")
+    context(0)
+    phase("y4")
+    y_in(4)
+    far_in(3)
+    phase("y_wait0")
+    y_ready(0)
+    phase("ctx1")
+    context(1)
+    phase("far4")
+    far_in(4)
+    phase("y_wait1")
+    y_ready(1)
+    phase("ctx2")
+    context(2)
+    phase("far_wait")
+    far_ready()
+    phase("ctx3")
+    context(3)
+    phase("attend")
 
     inv_scale = HEAD_DIM**-0.5
 
-    def attend(par):
+    def attend(off):
+        to = xx(off)
         for h in range(2):
             cols = slice(h * 128, h * 128 + 128)
             vcols = slice(256 + h * 128, 256 + h * 128 + 128)
-            q = qbuf[par, :, cols]
-            s_win = dot_t(q, kbuf[:, cols]) * inv_scale + bias[h, par]
+            q = qbuf[to, :, cols]
+            s_win = dot_t(q, kbuf[:, cols]) * inv_scale + bias[h, to]
             s_ctx = dot_t(q, kvc[:, :, cols].reshape(1024, 128)) * inv_scale
             top = jnp.maximum(
                 jnp.max(s_win, axis=1, keepdims=True), jnp.max(s_ctx, axis=1, keepdims=True)
@@ -378,25 +475,43 @@
             mixed = dot(e_win.astype(BF16), vbuf[:, cols]) + dot(
                 e_ctx.astype(BF16), kvc[:, :, vcols].reshape(1024, 128)
             )
-            att[par, :, cols] = (mixed / norm).astype(BF16)
-
-    attend(pc)
-    send(att.at[pc], attp, att_r, partner)
-    attend(c)
-    arrive(attp, att_r)
+            att[to, :, :, cols] = (mixed / norm).astype(BF16).reshape(2, 32, 128)
+        send(att.at[to, pc], attp.at[to], att_r.at[off], partner)
+
+    def finish(off):
+        to = xx(off)
+        arrive(attp.at[to], att_r.at[off])
+        mine_rows, other_rows = att[to, c], attp[to]
+
+        def out_cols(n, carry):
+            cols = pl.ds(pl.multiple_of(512 * n, 512), 512)
+            value = dot(mine_rows, wob[c, :, cols]) + dot(other_rows, wob[pc, :, cols])
+            obuf[to, :, cols] = value.astype(BF16)
+            return carry
+
+        lax.fori_loop(0, 4, out_cols, 0)
+        if off:
+            send(obuf.at[to], rbuf.at[off - 1], out_r.at[off - 1], (z, y, to, c))
+
+    attend(2)
     arrive(wob.at[pc], wo_r)
-
-    def out_cols(n, carry):
-        cols = pl.ds(pl.multiple_of(512 * n, 512), 512)
-        value = dot(att[c], wob[c, :, cols]) + dot(attp[...], wob[pc, :, cols])
-        obuf[:, :, cols] = value.astype(BF16).reshape(4, 32, 512)
-        return carry
-
-    lax.fori_loop(0, 4, out_cols, 0)
-    for dx in (2, 1, 3):
-        send(obuf.at[xx(dx)], rbuf.at[dx - 1], out_r.at[dx - 1], (z, y, xx(dx), c))
+    attend(1)
+    phase("finish2")
+    finish(2)
+    phase("attend3")
+    attend(3)
+    phase("finish1")
+    finish(1)
+    phase("attend0")
+    attend(0)
+    phase("finish3")
+    finish(3)
+    phase("finish0")
+    finish(0)
+    phase("out_wait")
     for dx in (1, 3, 2):
         arrive(rbuf.at[dx - 1], out_r.at[dx - 1])
+    phase("final")
     for j in range(16):
         cols = slice(j * 128, j * 128 + 128)
         branch = obuf[x, :, cols].astype(F32)
@@ -405,11 +520,13 @@
         out_ref[:, cols] = (
             latb[own_slot, :, cols].astype(F32) + gatev[j : j + 1, :] * branch
         ).astype(BF16)
+    phase("drain")
     for copy in sends:
         copy.wait_send()
-
-
-N_SENDS = 7 + 4 + 1 + 4 + 11 + 15 + 2 + 4 + 1 + 3 + 3 + 7 + 3 + 6 + 1 + 3
+    phase(None)
+
+
+N_SENDS = 19 + 8 + 22 + 10 + 4 + 10 + 9 + 9 + 15 + 1 + 4 + 3
 
 
 def on_device(
@@ -426,7 +543,7 @@
         out_specs=pl.BlockSpec(memory_space=pltpu.VMEM),
         scratch_shapes=[
             vm((16, 32, D), BF16),
-            vm((16, 2, 16, 1024), BF16),
+            vm((4, 2, 16, 16, 1024), BF16),
             vm((2, 16, 128), F32),
             vm((16, 128), F32),
             vm((3, 128, 256), BF16),
@@ -436,8 +553,8 @@
             vm((2, 256, D), BF16),
             vm((2, 16, 128), F32),
             vm((16, 128), F32),
-            vm((7, 16, 128), F32),
-            vm((16, 128), F32),
+            vm((7, 16, 128), BF16),
+            vm((16, 128), BF16),
             vm((2, 16, 128), F32),
             vm((16, 128), F32),
             vm((3, 16, 128), F32),
@@ -446,17 +563,17 @@
             vm((2, 16, 128), F32),
             vm((16, 128), F32),
             vm((512, 128), F32),
-            vm((256, 128), F32),
+            vm((1024, 128), F32),
             vm((512, D), BF16),
             vm((256, D), BF16),
-            vm((2, 128, 256), BF16),
+            vm((4, 64, 256), BF16),
             vm((512, 256), BF16),
             vm((512, 256), BF16),
             vm((4, 256, 512), BF16),
             vm((15, 4, 32, 128), F32),
-            vm((2, 2, 128, 512), F32),
-            vm((2, 128, 256), BF16),
-            vm((128, 256), BF16),
+            vm((2, 4, 64, 512), F32),
+            vm((4, 2, 32, 256), BF16),
+            vm((4, 32, 256), BF16),
             vm((4, 32, D), BF16),
             vm((3, 32, D), BF16),
             dma((14,)),
@@ -466,11 +583,14 @@
             dma((3,)),
             dma((8,)),
             dma((16,)),
-            dma((16,)),
-            dma((16,)),
+            dma((16, 2)),
+            dma((5,)),
+            dma((2, 5)),
+            dma((2, 5)),
+            dma((2, 5)),
+            dma((2, 5)),
             dma(()),
-            dma((6,)),
-            dma(()),
+            dma((4,)),
             dma((3,)),
         ],
         compiler_params=pltpu.CompilerParams(

time: 65.5 us -> 64.5 us (0.985)
  Pallas kernels: 62.2 us -> 61.2 us
    pallas_call x1, Pallas kernels: 62.2 us -> 61.2 us  [on_device(): pl.pallas_call(kernel, out_shape=jax.ShapeDtypeStruct((32, D), BF16), in_...]
where the time goes in v2:
time: 64.5 us; the launch traced here: 64.4 us
  Pallas kernels  61.2 us (95%)
  local copies, waits for them, and re-layouts  3.18 us (5%)
    pallas_call x1, Pallas kernels, on_device(): pl.pallas_call(kernel, out_shape=jax.ShapeDtypeStruct((32, D), BF16), in_...  61.2 us
    unnamed x2, local copies, waits for them, and re-layouts  2.51 us

profile of v2, /device:TPU:1, one launch (start us, length us, event | category | flops | bytes accessed | tf_op | source)
XLA Modules:
  0.0 64.4 jit_solution(4869706221844741668)
XLA Ops:
  0.0 0.9 %copy.14 = f32[16,15,31]{2,1,0:T(8,128)S(1)} copy(f32[16,15,31]{2,0,1:T(8,128)} %param.25) | data formatting | bytes 59520 | tf_op args[12]
  0.9 0.7 %pad.4.rb_hbm = f32[16,16,128]{2,1,0:T(8,128)} pad(f32[16,15,31]{2,1,0:T(8,128)S(1)} %copy.14, f32[]{:T(128)} %constant.2.clone.1), padding=0_0x0_1x0_97 | pad | bytes 160836 | tf_op jit(solution)/shard_map/jit(_pad)/pad | solution.py:538
  1.6 61.2 %whole_step.1 = bf16[32,2048]{1,0:T(8,128)(2,1)} custom-call(bf16[32,2048]{1,0:T(8,128)(2,1)} %lat_hbm.1, bf16[16,2048]{1,0:T(8,128)(2,1)} %ctx_hbm.1, f32[16,128]{1,0:T(8,128)} %bitcast.3, f32[16,128]{1,0:T(8,128)} %bitcast.4, f32[16,128]{1,0:T(8,128)} %bitcast.5, bf16[32,256]{1,0:T(8,128)(2,1)} %wsh_hbm.1, bf16[32,256]{1,0:T(8,128)(2,1)} %wsc_hbm.1, ...), custom_call_target="tpu_custom_call" | custom-call | tf_op jit(solution)/shard_map/whole_step/pallas_call | solution.py:539
  62.8 1.6 %copy.16 = bf16[32,2048]{1,0:T(8,128)(2,1)} copy(bf16[32,2048]{1,0:T(8,128)(2,1)} %whole_step.1) | data formatting | bytes 262144

commit v3 on v2

v3 whole, which is shorter than its diff:
```python
import jax
import jax.numpy as jnp
from jax import lax
from jax.experimental import pallas as pl
from jax.experimental.pallas import tpu as pltpu
from jax.sharding import Mesh
from jax.sharding import PartitionSpec as P

HEADS = 16
HEAD_DIM = 128
GRID_W = 32
WIN_H = 8
WIN_W = 16
NORM_EPS = 1e-06
NEG_BIG = -1e30
NZ, NY, NX, NC = 16, 4, 4, 2
NSP = NZ * NY
GRID_R = 512
D = 2048
F32 = jnp.float32
BF16 = jnp.bfloat16
A_OFFS = (4, -3, 3, -2, 2, -1, 1)
B_OFFS = (4, -4)
GROUPS = ((0, 1), (1, 5), (5, 9), (9, 13), (13, 16))


def dot(a, b):
    return jnp.dot(a, b, preferred_element_type=F32)


def dot_t(a, b):
    return lax.dot_general(a, b, (((1,), (1,)), ((), ())), preferred_element_type=F32)


def silu(v):
    return v / (1.0 + jnp.exp(-v))


def kernel(
    lat_hbm, ctx_hbm, cond_hbm, cctx_hbm, gain_hbm, wsh_hbm, wsc_hbm, wga_hbm,
    wq_hbm, wk_hbm, wv_hbm, wo_hbm, rb_hbm, out_ref,
    latb, ctxb, condv, gainv, wmod, w3, wob, rbv,
    pbuf, abuf, sbuf, bbuf, tbuf, cbuf, mod,
    gmv, shv, gatev, rl, rc, xn, xc, qbuf, kbuf, vbuf, kvc, rolled, bias,
    att, attp, obuf, mbuf, ubuf, fin,
    ld, snd, mod_r, ring_r, own_r, y_r, y_p, far_r, far_p, lat_r, end_r,
):
    z, y, x, c = (lax.axis_index(name) for name in ("z", "y", "x", "c"))
    t = x * 2 + c
    sp = z * NY + y
    pc = 1 - c

    def zz(d):
        return lax.rem(z + (NZ + d), NZ)

    def yy(d):
        return lax.rem(y + (NY + d), NY)

    def xx(d):
        return lax.rem(x + (NX + d), NX)

    def spd(d):
        other = lax.rem(sp + (NSP + d), NSP)
        return (other // NY, lax.rem(other, NY), x, c)

    def send(src, dst, kind, rsem, dev):
        pltpu.make_async_remote_copy(
            src_ref=src, dst_ref=dst, send_sem=snd.at[kind], recv_sem=rsem,
            device_id=dev, device_id_type=pl.DeviceIdType.MESH,
        ).start()

    partner = (z, y, x, pc)
    left, right = (z, y, xx(-1), c), (z, y, xx(1), c)

    def wait(view, sem):
        pltpu.make_async_copy(view, view, sem).wait()

    scope = []

    def phase(name):
        if scope:
            scope.pop().__exit__(None, None, None)
        if name:
            scope.append(jax.named_scope(name))
            scope[0].__enter__()

    phase("greet")
    barrier = pltpu.get_barrier_semaphore()
    greet = [(zz(d), y, x, c) for d in (1, 2, 3, 4, -1, -2, -3, -4)]
    greet += [(z, yy(d), x, c) for d in (1, 2, 3)]
    greet += [
        (z, y, xx(dx), c if dc == 0 else pc) for dx in range(4) for dc in range(2) if dx or dc
    ]
    greet += [spd(1), spd(-1)]
    for dev in greet:
        pl.semaphore_signal(barrier, inc=1, device_id=dev, device_id_type=pl.DeviceIdType.MESH)

    wmod[...] = jnp.zeros_like(wmod)
    mine = pl.ds(pl.multiple_of(y * 32, 32), 32)
    loads = [
        (cond_hbm, condv.at[0], 0),
        (cctx_hbm, condv.at[1], 0),
        (wsh_hbm, wmod.at[0, mine, :], 1),
        (wsc_hbm, wmod.at[1, mine, :], 1),
        (wga_hbm, wmod.at[2, mine, :], 1),
        (lat_hbm, latb.at[4 + t], 2),
        (ctx_hbm.at[:, pl.ds(0, 1024)], ctxb.at[0, 0, 0], 3),
        (ctx_hbm.at[:, pl.ds(1024, 1024)], ctxb.at[0, 1, 0], 3),
        (rb_hbm, rbv, 4),
        (wo_hbm, wob.at[c], 5),
        (gain_hbm, gainv, 6),
        (wk_hbm, w3.at[0], 7),
        (wv_hbm, w3.at[1], 7),
        (wq_hbm, w3.at[2], 7),
    ]
    for src, dst, k in loads:
        pltpu.make_async_copy(src, dst, ld.at[k]).start()

    phase("mod_load")
    wait(condv, ld.at[0])
    wait(wmod.at[:, mine, :], ld.at[1])
    phase("mod_term")
    lane = lax.broadcasted_iota(jnp.int32, (8, 128), 1)
    row = lax.broadcasted_iota(jnp.int32, (8, 128), 0)
    keep = (lane >= y * 32) & (lane < y * 32 + 32)
    a0 = jnp.where(keep, silu(condv[0, pl.ds(z, 1), :]), 0.0)
    a1 = jnp.where(keep, silu(condv[1, pl.ds(z, 1), :]), 0.0)
    total = None
    for i in range(3):
        lhs = jnp.where(row == 2 * i, a0, 0.0)
        if i < 2:
            lhs = jnp.where(row == 2 * i + 1, a1, lhs)
        term = dot(lhs.astype(BF16), wmod[i])
        total = term if total is None else total + term
    pbuf[0:8, :] = total[:, :128]
    pbuf[8:16, :] = total[:, 128:]
    phase("wait_barrier")
    wait(latb.at[4 + t], ld.at[2])
    wait(ctxb.at[0, :, 0], ld.at[3])
    pl.semaphore_wait(barrier, len(greet))

    phase("send_first")
    for k in range(3):
        send(pbuf, cbuf.at[k], 0, mod_r.at[0], (z, yy(k + 1), x, c))

    def piece(r, half, lo, hi):
        return ctxb.at[r, half, pl.ds(lo, hi - lo)]

    def ring(slot, sub, d):
        far = (slot + 1) // 2 + abs(d)
        to = 2 * far - 1 if d > 0 else 2 * far
        cols = pl.ds(512 * sub, 512)
        send(
            ctxb.at[0, c, slot, :, cols], ctxb.at[0, c, to, :, cols],
            2, ring_r.at[far - 1, sub], (zz(d), y, x, c),
        )

    def ring_in(near, sub):
        lo, hi = 2 * near - 1, min(2 * near + 1, 16)
        wait(ctxb.at[0, c, pl.ds(lo, hi - lo), :, pl.ds(512 * sub, 512)], ring_r.at[near - 1, sub])

    def ring_group(g):
        near = 2 * g
        for sub in range(2):
            ring_in(near, sub)
            if g < 4:
                ring(2 * near - 1, sub, 2)
                if g < 3:
                    ring(2 * near, sub, -2)
        if g < 4:
            for sub in range(2):
                ring(2 * near - 1, sub, 1)
                ring(2 * near, sub, -1)
        for sub in range(2):
            ring_in(near - 1, sub)
        y_out(g)
        own = piece(0, c, *GROUPS[g])
        send(own, own, 4, own_r.at[g // 3], partner)

    def y_out(g):
        for k in range(2):
            send(
                piece(0, c, *GROUPS[g]), piece(1 + k, c, *GROUPS[g]), 3, y_r.at[g],
                (z, yy(1 if k == 0 else -1), x, c),
            )

    def y_in(g):
        lo, hi = GROUPS[g]
        mid = (lo + hi + (g == 0)) // 2
        wait(ctxb.at[pl.ds(1, 2), c, pl.ds(lo, hi - lo)], y_r.at[g])
        for k, (first, last) in enumerate(((lo, mid), (mid, hi))):
            if last > first:
                send(
                    piece(1 + k, c, first, last), piece(3, c, first, last), 6, far_r.at[g],
                    (z, yy(1 if k == 0 else -1), x, c),
                )
        for k in range(2):
            got = piece(1 + k, c, lo, hi)
            send(got, got, 5, y_p.at[g // 3], partner)

    def far_in(g):
        got = piece(3, c, *GROUPS[g])
        wait(got, far_r.at[g])
        send(got, got, 6, far_p.at[g // 3], partner)

    def lat_send(slot, rsem, dev):
        send(latb.at[slot], latb.at[slot], 7, rsem, dev)

    own_slot = 4 + t
    halo_slot = lax.rem(t + 12, 16)

    def slot_of(kind, dx, core):
        other = xx(dx) * 2 + core
        return 4 + other if kind == 0 else lax.rem(other + 12, 16)

    def lat_out(kind):
        slot = slot_of(kind, 0, c)
        lat_send(slot, lat_r.at[1 + kind], right)
        lat_send(slot, lat_r.at[1 + kind], left)
        lat_send(slot, lat_r.at[5], partner)

    def lat_near(kind):
        wait(latb.at[pl.ds(0, 2)], lat_r.at[1 + kind])
        for dx, lo, dev in ((-1, 0, right), (1, 16, left)):
            part = latb.at[slot_of(kind, dx, c), pl.ds(lo, 16)]
            send(part, part, 7, lat_r.at[3 + kind], dev)
        for dx in (-1, 1):
            lat_send(slot_of(kind, dx, c), lat_r.at[5], partner)

    def lat_far(kind):
        slot = slot_of(kind, 2, c)
        wait(latb.at[slot], lat_r.at[3 + kind])
        lat_send(slot, lat_r.at[5], partner)

    for d in (2, 1):
        for sub in range(2):
            for sign in (1, -1):
                ring(0, sub, d * sign)
    y_out(0)
    to_prev = x < 2
    spn = lax.rem(sp + jnp.where(to_prev, NSP - 1, 1), NSP)
    send(
        latb.at[own_slot], latb.at[halo_slot], 7, lat_r.at[0],
        (spn // NY, lax.rem(spn, NY), x, c),
    )
    lat_out(0)

    row32 = lax.broadcasted_iota(jnp.int32, (32, 128), 0)
    lane32 = lax.broadcasted_iota(jnp.int32, (32, 128), 1)
    c2 = lax.rem(lane32, 32)
    b0 = jnp.clip(row32 - WIN_W // 2, 0, GRID_W - WIN_W)
    col_in = (c2 >= b0) & (c2 < b0 + WIN_W)
    quarter = lane32 // 32

    def bias_head(h):
        def roll_e(e, inner):
            line = rbv[e, pl.ds(2 * t + h, 1), :]
            line = jnp.concatenate([line, jnp.zeros((1, 97), F32)], axis=1)
            line = jnp.broadcast_to(line, (32, 128))
            for k in range(4):
                rolled[e, k] = pltpu.roll(line, (32 * k + 113) % 128, 1, stride=1, stride_axis=0)
            return inner

        lax.fori_loop(0, 15, roll_e, 0)
        for i in range(8):
            first = sp * 8
            start = jnp.clip(first + i - WIN_H // 2, 0, GRID_R - WIN_H) - first + 4
            for q in range(4):
                tile = jnp.full((32, 128), NEG_BIG, F32)
                for k in range(4):
                    e = 4 * q + k - i + 3
                    if 0 <= e < 15:
                        tile = jnp.where(quarter == k, rolled[e, k], tile)
                j = 4 * q + quarter
                ok = col_in & (j >= start) & (j < start + WIN_H)
                bias[h, i % 2, (i // 2) * 32 : (i // 2) * 32 + 32, q * 128 : q * 128 + 128] = (
                    jnp.where(ok, tile, NEG_BIG)
                )

    phase("bias0")
    wait(rbv, ld.at[4])
    bias_head(0)

    phase("mod_y")
    wait(cbuf, mod_r.at[0])
    sbuf[...] = (pbuf[...] + cbuf[0] + cbuf[1] + cbuf[2]).astype(BF16)
    for k, d in enumerate(A_OFFS):
        send(sbuf, abuf.at[k], 1, mod_r.at[1], (zz(d), y, x, c))

    phase("ring1")
    ring_group(1)
    phase("halo")
    wait(latb.at[halo_slot], lat_r.at[0])
    lat_out(1)
    wait(wob.at[c], ld.at[5])
    send(wob.at[c], wob.at[c], 8, end_r.at[0], partner)
    phase("bias1")
    bias_head(1)
    phase("y0")
    y_in(0)
    phase("lat_own")
    lat_near(0)

    phase("mod_a")
    wait(abuf, mod_r.at[1])
    part = sbuf[...].astype(F32)
    for k in range(7):
        part = part + abuf[k].astype(F32)
    tbuf[...] = part
    for k, d in enumerate(B_OFFS):
        send(tbuf, bbuf.at[k], 0, mod_r.at[2], (zz(d), y, x, c))

    phase("ring2")
    ring_group(2)
    phase("y1")
    y_in(1)
    far_in(0)
    phase("lat_halo")
    lat_near(1)
    lat_far(0)

    phase("ring3")
    ring_group(3)
    phase("mod_b")
    wait(bbuf, mod_r.at[2])
    mod[t] = bbuf[0] + bbuf[1]
    for dx in (2, 1, 3, 0):
        for dc in range(2):
            if dx or dc:
                send(
                    mod.at[t], mod.at[t], 0, mod_r.at[3],
                    (z, y, xx(dx), c if dc == 0 else pc),
                )

    phase("y2")
    y_in(2)
    far_in(1)
    phase("lat_far")
    lat_far(1)

    def ctx_tile(g, j):
        block = ctxb[
            g // 2, j // 8, pl.ds(8 * lax.rem(g, 2), 8), :, (j % 8) * 128 : (j % 8) * 128 + 128
        ]
        return block.reshape(128, 128).astype(F32)

    def lat_tile(g, j):
        return latb[pl.ds(4 * g, 4), :, j * 128 : j * 128 + 128].reshape(128, 128).astype(F32)

    def stats(tile_of, dest, first, count, step_by=1):
        def step(i, carry):
            g = first + i * step_by
            acc = jnp.zeros((128, 128), F32)
            for j in range(16):
                tile = tile_of(g, j)
                acc = acc + tile * tile
            mean = jnp.sum(acc, axis=1, keepdims=True) * (1.0 / D)
            dest[pl.ds(pl.multiple_of(128 * g, 128), 128), :] = jnp.broadcast_to(
                lax.rsqrt(mean + NORM_EPS), (128, 128)
            )
            return carry

        lax.fori_loop(0, count, step, 0)

    phase("stats_ctx")
    wait(ctxb.at[0, pc, pl.ds(1, 8)], own_r.at[0])
    wait(ctxb.at[pl.ds(1, 2), pc, pl.ds(0, 9)], y_p.at[0])
    stats(ctx_tile, rc, 0, 3, 2)
    phase("ring4")
    ring_group(4)
    phase("lat_parts")
    wait(latb.at[pl.ds(0, 8)], lat_r.at[5])
    phase("stats_lat")
    stats(lat_tile, rl, 0, 4)
    phase("y3")
    y_in(3)
    far_in(2)
    phase("mod_gather")
    wait(gainv, ld.at[6])
    wait(w3, ld.at[7])
    wait(rl.at[pl.ds(0, 112)], mod_r.at[3])
    phase("mod_rows")
    for j in range(16):
        low = (j % 2) * 8
        for which in range(2):
            gmv[which, j : j + 1, :] = gainv[j : j + 1, :] * (
                1.0 + mod[j // 2, low + 2 + which : low + 3 + which, :]
            )
            shv[which, j : j + 1, :] = mod[j // 2, low + which : low + which + 1, :]
        gatev[j : j + 1, :] = mod[j // 2, low + 4 : low + 5, :]

    def normed(tile_of, scale, which, dest, first, count):
        def step(g, carry):
            rows = pl.ds(pl.multiple_of(128 * g, 128), 128)
            to = pl.ds(pl.multiple_of(128 * (g - first), 128), 128)
            inv = scale[rows, :]
            for j in range(16):
                value = tile_of(g, j) * inv * gmv[which, j : j + 1, :] + shv[which, j : j + 1, :]
                dest[to, j * 128 : j * 128 + 128] = value.astype(BF16)
            return carry

        lax.fori_loop(first, first + count, step, 0)

    def project(g, carry):
        rows = pl.ds(pl.multiple_of(256 * g, 256), 256)
        kbuf[rows, :] = dot(xn[rows, :], w3[0]).astype(BF16)
        vbuf[rows, :] = dot(xn[rows, :], w3[1]).astype(BF16)
        return carry

    def context(r):
        normed(ctx_tile, rc, 1, xc, 2 * r, 2)
        kvc[r, :, 0:256] = dot(xc[...], w3[0]).astype(BF16)
        kvc[r, :, 256:512] = dot(xc[...], w3[1]).astype(BF16)

    phase("lat_norm")
    normed(lat_tile, rl, 0, xn, 0, 4)
    phase("lat_proj")
    lax.fori_loop(0, 2, project, 0)
    phase("lat_q")
    queries = dot(xn[128:384, :], w3[2]).astype(BF16)
    for i in range(8):
        qbuf[i % 2, (i // 2) * 32 : (i // 2) * 32 + 32, :] = queries[i * 32 : i * 32 + 32, :]
    phase("y4")
    y_in(4)
    far_in(3)
    phase("own_wait")
    wait(ctxb.at[0, pc, pl.ds(9, 7)], own_r.at[1])
    phase("ctx0")
    stats(ctx_tile, rc, 1, 1)
    context(0)
    phase("y_wait")
    wait(ctxb.at[pl.ds(1, 2), pc, pl.ds(9, 7)], y_p.at[1])
    phase("ctx1")
    stats(ctx_tile, rc, 3, 2, 2)
    context(1)
    phase("far4")
    far_in(4)
    phase("ctx2")
    context(2)
    phase("far_wait")
    wait(ctxb.at[3, pc, pl.ds(0, 9)], far_p.at[0])
    wait(ctxb.at[3, pc, pl.ds(9, 7)], far_p.at[1])
    phase("ctx3")
    stats(ctx_tile, rc, 6, 2)
    context(3)

    inv_scale = HEAD_DIM**-0.5

    def attend(par):
        for h in range(2):
            cols = slice(h * 128, h * 128 + 128)
            vcols = slice(256 + h * 128, 256 + h * 128 + 128)
            q = qbuf[par, :, cols]
            s_win = dot_t(q, kbuf[:, cols]) * inv_scale + bias[h, par]
            s_ctx = dot_t(q, kvc[:, :, cols].reshape(1024, 128)) * inv_scale
            top = jnp.maximum(
                jnp.max(s_win, axis=1, keepdims=True), jnp.max(s_ctx, axis=1, keepdims=True)
            )
            e_win = jnp.exp(s_win - top)
            e_ctx = jnp.exp(s_ctx - top)
            norm = jnp.sum(e_win, axis=1, keepdims=True) + jnp.sum(e_ctx, axis=1, keepdims=True)
            mixed = dot(e_win.astype(BF16), vbuf[:, cols]) + dot(
                e_ctx.astype(BF16), kvc[:, :, vcols].reshape(1024, 128)
            )
            att[par, :, cols] = (mixed / norm).astype(BF16)

    phase("attend")
    attend(pc)
    send(att.at[pc], attp, 9, end_r.at[1], partner)
    attend(c)
    phase("att_wait")
    wait(wob.at[pc], end_r.at[0])
    wait(attp, end_r.at[1])

    def out_cols(n, carry):
        cols = pl.ds(pl.multiple_of(512 * n, 512), 512)
        value = dot(att[c], wob[c, :, cols]) + dot(attp[...], wob[pc, :, cols])
        obuf[:, :, cols] = value.astype(BF16).reshape(4, 32, 512)
        return carry

    low_cols, high_cols = pl.ds(0, 1024), pl.ds(1024, 1024)

    def give(dest, cols, to, dev):
        send(obuf.at[dest, :, cols], to, 10, end_r.at[4], dev)

    phase("out_low")
    lax.fori_loop(0, 2, out_cols, 0)
    send(obuf.at[xx(2), :, low_cols], mbuf.at[0], 10, end_r.at[2], right)
    give(xx(-1), low_cols, fin.at[1, :, low_cols], left)
    phase("out_high")
    lax.fori_loop(2, 4, out_cols, 0)
    send(obuf.at[xx(2), :, high_cols], mbuf.at[1], 10, end_r.at[3], left)
    give(xx(1), high_cols, fin.at[0, :, high_cols], right)
    phase("out_sum")
    for k, cols, dx, dev in ((0, low_cols, 1, right), (1, high_cols, -1, left)):
        wait(mbuf.at[k], end_r.at[2 + k])
        ubuf[k] = (obuf[xx(dx), :, cols].astype(F32) + mbuf[k].astype(F32)).astype(BF16)
        send(ubuf.at[k], fin.at[k, :, cols], 10, end_r.at[4], dev)
    phase("out_wait")
    wait(fin, end_r.at[4])
    phase("final")
    for j in range(16):
        cols = slice(j * 128, j * 128 + 128)
        branch = (
            obuf[x, :, cols].astype(F32) + fin[0, :, cols].astype(F32) + fin[1, :, cols].astype(F32)
        )
        out_ref[:, cols] = gatev[j : j + 1, :] * branch
    phase("drain")
    slots = ctxb.at[0, 0, pl.ds(1, 15)]
    for k, view in enumerate((
        rl.at[pl.ds(0, 192)], abuf, slots, ctxb.at[0], slots, ctxb.at[0], ctxb.at[0],
        latb.at[pl.ds(0, 15)], wob.at[0], attp, latb.at[pl.ds(0, 3)],
    )):
        wait(view, snd.at[k])
    phase(None)


def on_device(
    latent, context, condition, ctx_cond, norm_gain, w_shift, w_scale, w_gate,
    w_query, w_key, w_value, w_out, rel_bias,
):
    vm = pltpu.VMEM
    dma = pltpu.SemaphoreType.DMA
    delta = pl.pallas_call(
        kernel,
        out_shape=jax.ShapeDtypeStruct((32, D), F32),
        in_specs=[pl.BlockSpec(memory_space=pl.ANY)] * 13,
        out_specs=pl.BlockSpec(memory_space=pltpu.VMEM),
        scratch_shapes=[
            vm((16, 32, D), BF16),
            vm((4, 2, 16, 16, 1024), BF16),
            vm((2, 16, 128), F32),
            vm((16, 128), F32),
            vm((3, 128, 256), BF16),
            vm((3, D, 256), BF16),
            vm((2, 256, D), BF16),
            vm((15, 16, 31), F32),
            vm((16, 128), F32),
            vm((7, 16, 128), BF16),
            vm((16, 128), BF16),
            vm((2, 16, 128), F32),
            vm((16, 128), F32),
            vm((3, 16, 128), F32),
            vm((8, 16, 128), F32),
            vm((2, 16, 128), F32),
            vm((2, 16, 128), F32),
            vm((16, 128), F32),
            vm((512, 128), F32),
            vm((1024, 128), F32),
            vm((512, D), BF16),
            vm((256, D), BF16),
            vm((2, 128, 256), BF16),
            vm((512, 256), BF16),
            vm((512, 256), BF16),
            vm((4, 256, 512), BF16),
            vm((15, 4, 32, 128), F32),
            vm((2, 2, 128, 512), F32),
            vm((2, 128, 256), BF16),
            vm((128, 256), BF16),
            vm((4, 32, D), BF16),
            vm((2, 32, 1024), BF16),
            vm((2, 32, 1024), BF16),
            vm((2, 32, D), BF16),
            dma((8,)),
            dma((11,)),
            dma((4,)),
            dma((8, 2)),
            dma((2,)),
            dma((5,)),
            dma((2,)),
            dma((5,)),
            dma((2,)),
            dma((6,)),
            dma((5,)),
        ],
        compiler_params=pltpu.CompilerParams(
            collective_id=0, has_side_effects=True, vmem_limit_bytes=56 * 1024 * 1024
        ),
        name="whole_step",
    )(
        latent, context, condition.reshape(16, 128), ctx_cond.reshape(16, 128),
        norm_gain.reshape(16, 128), w_shift, w_scale, w_gate, w_query, w_key, w_value, w_out,
        jnp.transpose(rel_bias, (1, 0, 2)),
    )
    return (latent.astype(F32) + delta).astype(BF16)


def solution(mesh):
    torus = Mesh(mesh.devices.reshape(NZ, NY, NX, NC), ("z", "y", "x", "c"))
    sp, tp = ("z", "y"), ("x", "c")
    return jax.shard_map(
        on_device,
        mesh=torus,
        in_specs=(
            P((*sp, *tp), None),
            P(sp, None),
            P(),
            P(),
            P(),
            P(sp, tp),
            P(sp, tp),
            P(sp, tp),
            P(None, tp),
            P(None, tp),
            P(None, tp),
            P(tp, None),
            P(),
        ),
        out_specs=P((*sp, *tp), None),
        check_vma=False,
    )
```

time: 64.5 us -> 58.9 us (0.913)
  Pallas kernels: 61.2 us -> 57.1 us
  local copies, waits for them, and re-layouts: 3.18 us -> 0.01 us
  other arithmetic: 0 us -> 1.63 us
    pallas_call x1, Pallas kernels: 61.2 us -> 57.1 us  [on_device(): pl.pallas_call(kernel, out_shape=jax.ShapeDtypeStruct((32, D), F32), in_s...]
    unnamed x2, local copies, waits for them, and re-layouts: 2.51 us -> 0.01 us
    convert_element_type x0 -> x1, other arithmetic: none -> 1.63 us  [on_device(): return (latent.astype(F32) + delta).astype(BF16)]
    pad x1 -> x0, local copies, waits for them, and re-layouts: 0.67 us -> none  [on_device(): bias_rows = jnp.pad(rel_bias, ((0, 0), (0, 1), (0, 97)))]
where the time goes in v3:
time: 58.9 us; the launch traced here: 58.8 us
  Pallas kernels  57.1 us (97%)
  other arithmetic  1.63 us (3%)
    pallas_call x1, Pallas kernels, on_device(): pl.pallas_call(kernel, out_shape=jax.ShapeDtypeStruct((32, D), F32), in_s...  57.1 us
    convert_element_type x1, other arithmetic, on_device(): return (latent.astype(F32) + delta).astype(BF16)  1.63 us

profile of v3, /device:TPU:1, one launch (start us, length us, event | category | flops | bytes accessed | tf_op | source)
XLA Modules:
  0.0 58.8 jit_solution(14741802122629824715)
XLA Ops:
  0.0 0.0 copy-start
  0.0 57.1 %whole_step.1 = f32[32,2048]{1,0:T(8,128)} custom-call(bf16[32,2048]{1,0:T(8,128)(2,1)} %lat_hbm.1, bf16[16,2048]{1,0:T(8,128)(2,1)} %ctx_hbm.1, f32[16,128]{1,0:T(8,128)} %bitcast.5, f32[16,128]{1,0:T(8,128)} %bitcast.6, f32[16,128]{1,0:T(8,128)} %bitcast.7, bf16[32,256]{1,0:T(8,128)(2,1)} %wsh_hbm.1, bf16[32,256]{1,0:T(8,128)(2,1)} %wsc_hbm.1, ...), custom_call_target="tpu_custom_call" | custom-call | tf_op jit(solution)/shard_map/whole_step/pallas_call | solution.py:524
  57.1 0.0 copy-done
  57.2 1.6 %add_convert_fusion = bf16[32,2048]{1,0:T(8,128)(2,1)} fusion(f32[32,2048]{1,0:T(8,128)} %whole_step.1, bf16[32,2048]{1,0:T(8,128)(2,1)S(1)} %copy-done), kind=kLoop, calls=%fused_computation | loop fusion | flops 196608 | bytes 524288 | tf_op jit(solution)/shard_map/convert_element_type | solution.py:585
Async XLA Ops:
  0.0 57.1 %copy-start = (bf16[32,2048]{1,0:T(8,128)(2,1)S(1)}, bf16[32,2048]{1,0:T(8,128)(2,1)}, u32[]{:S(2)}) copy-start(bf16[32,2048]{1,0:T(8,128)(2,1)} %lat_hbm.1) | copy-start | bytes 393220
